TPU v7x, 32 devices: a whole 2x2x4 slice. The times are simulated.
32 devices in a mesh: ep: 4 (over y, x), tp: 8 (over z, core).
Axes of the slice: x: 2, y: 2, z: 4, core: 2. Of those that a mesh axis runs over, the one named last changes fastest.
Arguments:
- pool_input: bfloat16 [4096, 1024], P('ep', 'tp'), may hold values from -6 to 6
- pool_gain: float32 [1024], P('tp'), may hold values from 0.1 to 1.9
- mix_weight: bfloat16 [1024, 2048], P('tp'), may hold values from -0.1875 to 0.1875
- moe_input: bfloat16 [8192, 2048], P(('ep', 'tp')), may hold values from -6 to 6
- moe_gain: float32 [2048], replicated, may hold values from 0.1 to 1.9
- expert_ids: int32 [8192, 2], P(('ep', 'tp')), may hold values from 0 to 15, as said below
- route_weight: float32 [8192, 2], P(('ep', 'tp')), may hold values from 0.2 to 1
- gate_weight: bfloat16 [16, 2048, 1024], P('ep', None, 'tp'), may hold values from -0.125 to 0.125
- up_weight: bfloat16 [16, 2048, 1024], P('ep', None, 'tp'), may hold values from -0.125 to 0.125
- down_weight: bfloat16 [16, 2048, 1024], P('ep', None, 'tp'), may hold values from -0.1875 to 0.1875
Outputs:
- mixed_out: bfloat16 [4096, 2048], P(('ep', 'tp'))
- moe_out: bfloat16 [8192, 2048], P(('ep', 'tp'))
Inputs may be any that keep to these rules, and one draw needn't show every extreme that they name: `expert_ids`: each row names 2 different experts of one group of 4 consecutive experts. In each aligned block of 256 rows (the rows of one device) no expert is named by more than 48 rows, and some expert is named by exactly 48 rows.
All inputs are finite; a program needn't handle non-finite values.
Results may differ from a plain program's by a relative error of at most 0.012.
Values may be sent and summed in bfloat16 or wider, within the bound.
A program may use at most 128 MiB of HBM per device.

v0:
```python
import jax
import jax.numpy as jnp
from jax import lax
from jax.sharding import PartitionSpec as P

GROUP_CH = 256
EXPERTS = 16
GROUP_EXP = 4
TOP = 2
CAP = 48
CHUNKS = 2


eps_norm = 1e-06


def from_behind(shard, axis, by):
    peers = lax.axis_size(axis)
    pairs = [(i, i + by) for i in range(peers) if 0 <= i + by < peers]
    return lax.ppermute(shard, axis, pairs)


def window_sums(extended, row_count):
    level_sum = extended
    stride = 1
    outputs = []
    for doubling in range(4):
        level_sum = level_sum[stride:] + level_sum[:-stride]
        stride = stride * 2
        outputs.append(level_sum[level_sum.shape[0] - row_count :])
    return outputs


def pool_mixer(pool_input, pool_gain):
    row_count, channels = pool_input.shape
    carried = from_behind(pool_input[row_count - 15 :], "ep", 1)
    extended = jnp.concatenate([carried, pool_input], axis=0).astype(jnp.float32)
    window_list = window_sums(extended, row_count)
    channel_ids = lax.axis_index("tp") * channels + lax.iota(jnp.int32, channels)
    group_ids = channel_ids // GROUP_CH
    position = lax.axis_index("ep") * row_count + lax.iota(jnp.int32, row_count)
    summed = jnp.zeros((row_count, channels), jnp.float32)
    widths = jnp.zeros((channels,), jnp.int32)
    for index_group in range(4):
        inside = group_ids == index_group
        summed = jnp.where(inside[None, :], window_list[index_group], summed)
        widths = jnp.where(inside, 2 ** (index_group + 1), widths)
    counted = jnp.minimum(position[:, None] + 1, widths[None, :]).astype(jnp.float32)
    values = extended[15:]
    return ((summed / counted - values) * pool_gain).astype(jnp.bfloat16)


def dispatch_plan(expert_ids, route_weight, ep_size):
    local_experts = EXPERTS // ep_size
    share = TOP if local_experts % GROUP_EXP == 0 else 1
    capacity = local_experts * CAP // share
    owners = expert_ids // local_experts
    ep_index = lax.iota(jnp.int32, ep_size)
    member = jnp.any(owners[:, :, None] == ep_index[None, None, :], axis=1)
    counts = member.astype(jnp.int32)
    rank = jnp.cumsum(counts, axis=0) - counts
    slot = jnp.where(member, rank, -1).T
    placing = slot[:, None, :] == lax.iota(jnp.int32, capacity)[None, :, None]
    dense_weight = jnp.sum(
        jnp.where(
            expert_ids[:, :, None] == lax.iota(jnp.int32, EXPERTS)[None, None, :],
            route_weight[:, :, None],
            0.0,
        ),
        axis=1,
    )
    dense_weight = dense_weight.reshape(-1, ep_size, local_experts)
    slot_weight = jnp.einsum(
        "ecn,nej->ecj",
        placing.astype(jnp.float32),
        dense_weight,
        precision=lax.Precision.HIGHEST,
    )
    return placing.astype(jnp.bfloat16).reshape(ep_size * capacity, -1), slot_weight, capacity


def body(
    pool_input,
    pool_gain,
    mix_weight,
    moe_input,
    moe_gain,
    expert_ids,
    route_weight,
    gate_weight,
    up_weight,
    down_weight,
):
    pooled = pool_mixer(pool_input, pool_gain)
    ep_size = lax.axis_size("ep")
    out_columns = mix_weight.shape[1] // ep_size
    mix_columns = lax.dynamic_slice_in_dim(
        mix_weight, lax.axis_index("ep") * out_columns, out_columns, axis=1
    )
    mix_columns = lax.all_gather(mix_columns, "tp", axis=0, tiled=True)
    inputs = moe_input.astype(jnp.float32)
    scale_rows = lax.rsqrt(jnp.mean(inputs * inputs, axis=-1, keepdims=True) + eps_norm)
    normed = (inputs * scale_rows * moe_gain).astype(jnp.bfloat16)
    placing, slot_weight, capacity = dispatch_plan(expert_ids, route_weight, ep_size)
    rows = capacity // CHUNKS
    arrived_list = []
    placing_list = []
    for chunk in range(CHUNKS):
        chunk_placing = placing.reshape(ep_size, capacity, -1)[:, chunk * rows : (chunk + 1) * rows]
        chunk_placing = chunk_placing.reshape(ep_size * rows, -1)
        outgoing = jnp.dot(chunk_placing, normed, preferred_element_type=jnp.float32)
        outgoing = outgoing.astype(jnp.bfloat16)
        placing_list.append(chunk_placing)
        arrived_list.append(
            lax.all_to_all(outgoing, "ep", split_axis=0, concat_axis=0, tiled=True)
        )
    arrived_list[0], mix_columns = lax.optimization_barrier((arrived_list[0], mix_columns))
    weights = lax.all_to_all(slot_weight, "ep", split_axis=0, concat_axis=0, tiled=True)
    weights = lax.all_gather(weights, "tp", axis=0, tiled=True)
    combined = jnp.zeros(normed.shape, jnp.float32)
    for chunk in range(CHUNKS):
        tokens = lax.all_gather(arrived_list[chunk], "tp", axis=0, tiled=True)
        scales = weights[:, chunk * rows : (chunk + 1) * rows].reshape(tokens.shape[0], -1)
        gate_part = jnp.einsum(
            "nd,edf->enf", tokens, gate_weight, preferred_element_type=jnp.float32
        )
        upward = jnp.einsum("nd,edf->enf", tokens, up_weight, preferred_element_type=jnp.float32)
        hidden = (jax.nn.silu(gate_part) * upward * scales.T[:, :, None]).astype(jnp.bfloat16)
        partial = jnp.einsum("enf,edf->nd", hidden, down_weight, preferred_element_type=jnp.float32)
        reduced = lax.psum_scatter(
            partial.astype(jnp.bfloat16), "tp", scatter_dimension=0, tiled=True
        )
        returned = lax.all_to_all(reduced, "ep", split_axis=0, concat_axis=0, tiled=True)
        combined = combined + lax.dot_general(
            placing_list[chunk],
            returned,
            (((0,), (0,)), ((), ())),
            preferred_element_type=jnp.float32,
        )
    moe_out = combined.astype(jnp.bfloat16)
    regrouped = lax.all_to_all(pooled, "tp", split_axis=0, concat_axis=1, tiled=True)
    half = regrouped.shape[1] // 2
    mixed_sum = 0.0
    for part in range(2):
        section = slice(part * half, (part + 1) * half)
        pooled_rows = lax.all_gather(regrouped[:, section], "ep", axis=0, tiled=True)
        mixed_sum = mixed_sum + jnp.dot(
            pooled_rows, mix_columns[section], preferred_element_type=jnp.float32
        )
    mixed_out = lax.all_to_all(
        mixed_sum.astype(jnp.bfloat16), "ep", split_axis=0, concat_axis=1, tiled=True
    )
    return (mixed_out, moe_out)


def solution(mesh):
    return jax.shard_map(
        body,
        mesh=mesh,
        in_specs=(
            P("ep", "tp"),
            P("tp"),
            P("tp", None),
            P(("ep", "tp"), None),
            P(),
            P(("ep", "tp"), None),
            P(("ep", "tp"), None),
            P("ep", None, "tp"),
            P("ep", None, "tp"),
            P("ep", None, "tp"),
        ),
        out_specs=(P(("ep", "tp"), None), P(("ep", "tp"), None)),
        check_vma=False,
    )
```

profile of v0, /device:TPU:0, one launch (start us, length us, event | category | flops | bytes accessed | tf_op | source)
XLA Modules:
  0.0 334.8 jit_solution(6030024763773392144)
XLA Ops:
  7.3 1.7 constant_dynamic-slice_fusion
  9.1 0.7 and_select_fusion
  9.8 1.5 fusion.40
  11.3 1.2 reduce-window.6
  13.0 1.7 convolution_convert_fusion
  14.8 16.4 %all_to_all.85 = bf16[4,48,2048]{2,1,0:T(8,128)(2,1)} all-to-all(bf16[4,48,2048]{2,1,0:T(8,128)(2,1)S(1)} %bitcast.128), channel_id=1, replica_groups=mesh['ep'=4,'tp'=8] {'ep'}, dimensions={0} | all-to-all | bytes 1572864 | tf_op jit(solution)/shard_map/all_to_all | solution.py:115
  31.3 0.5 convolution_convert_fusion.1
  31.8 13.2 %all_to_all.86 = bf16[4,48,2048]{2,1,0:T(8,128)(2,1)} all-to-all(bf16[4,48,2048]{2,1,0:T(8,128)(2,1)S(1)} %bitcast.127), channel_id=1, replica_groups=mesh['ep'=4,'tp'=8] {'ep'}, dimensions={0} | all-to-all | bytes 1572864 | tf_op jit(solution)/shard_map/all_to_all | solution.py:115
  45.4 7.0 %all_to_all.87 = f32[4,96,4]{1,2,0:T(4,128)S(1)} all-to-all(f32[4,96,4]{1,2,0:T(4,128)S(1)} %fusion.65), channel_id=1, replica_groups=mesh['ep'=4,'tp'=8] {'ep'}, dimensions={0} | all-to-all | bytes 12288 | tf_op jit(solution)/shard_map/all_to_all | solution.py:118
  52.5 14.8 %all_gather.22 = f32[32,96,4]{1,2,0:T(4,128)S(1)} all-gather(f32[4,96,4]{1,2,0:T(4,128)S(1)} %all_to_all.87), channel_id=1, replica_groups=mesh['ep'=4,'tp'=8] {'tp'}, dimensions={0}, use_global_device_ids=true | all-gather | bytes 55296 | tf_op jit(solution)/shard_map/all_gather | solution.py:119
  67.5 34.2 %all-gather.8.cloned.1.call-done = bf16[1536,2048]{1,0:T(8,128)(2,1)} async-done(((bf16[192,2048]{1,0:T(8,128)(2,1)}), bf16[1536,2048]{1,0:T(8,128)(2,1)}) %all-gather.8.cloned.1.call-update) | async-done | bytes 6291472 | tf_op jit(solution)/shard_map/all_gather | solution.py:122
  101.7 8.5 %fusion.20 = f32[4,1536,128]{2,1,0:T(8,128)} fusion(bf16[4,2048,128]{2,1,0:T(8,128)(2,1)} %param.17, bf16[1536,2048]{1,0:T(8,128)(2,1)} %all-gather.8.cloned.1.call-done), kind=kOutput, calls=%fused_computation.14 | convolution fusion | flops 3221225472 | bytes 11534336 | tf_op jit(solution)/shard_map/nd,edf->enf/dot_general | solution.py:124
  110.2 12.3 %bitcast_convert_fusion = bf16[1536,2048]{1,0:T(8,128)(2,1)} fusion(bf16[4,2048,128]{2,1,0:T(8,128)(2,1)S(1)} %copy-done, bf16[4,2048,128]{2,1,0:T(8,128)(2,1)} %param.18, bf16[1536,2048]{1,0:T(8,128)(2,1)} %all-gather.8.cloned.1.call-done, f32[4,1536,128]{2,1,0:T(8,128)} %fusion.20, f32[4,1536]{1,0:T(4,128)S(1)} %bitcast.132), kind=kOutput, calls=%fused_computation | convolution fusion | flops 6451101696 | bytes 19947520 | tf_op jit(solution)/shard_map/enf,edf->nd/dot_general | solution.py:129
  122.9 43.8 %all-gather.6.cloned.1.call-done = bf16[1536,2048]{1,0:T(8,128)(2,1)} async-done(((bf16[192,2048]{1,0:T(8,128)(2,1)}), bf16[1536,2048]{1,0:T(8,128)(2,1)}) %all-gather.6.cloned.1.call-update) | async-done | bytes 6291472 | tf_op jit(solution)/shard_map/all_gather | solution.py:122
  166.7 8.5 %fusion.8 = f32[4,1536,128]{2,1,0:T(8,128)} fusion(bf16[4,2048,128]{2,1,0:T(8,128)(2,1)} %param.17, bf16[1536,2048]{1,0:T(8,128)(2,1)} %all-gather.6.cloned.1.call-done), kind=kOutput, calls=%fused_computation.10 | convolution fusion | flops 3221225472 | bytes 11534336 | tf_op jit(solution)/shard_map/nd,edf->enf/dot_general | solution.py:124
  175.3 11.8 %bitcast_convert_fusion.1 = bf16[1536,2048]{1,0:T(8,128)(2,1)} fusion(bf16[4,2048,128]{2,1,0:T(8,128)(2,1)S(1)} %copy-done, bf16[4,2048,128]{2,1,0:T(8,128)(2,1)} %param.18, bf16[1536,2048]{1,0:T(8,128)(2,1)} %all-gather.6.cloned.1.call-done, f32[4,1536,128]{2,1,0:T(8,128)} %fusion.8, f32[4,1536]{1,0:T(4,128)S(1)} %bitcast.133), kind=kOutput, calls=%fused_computation.1 | convolution fusion | flops 6451101696 | bytes 19947520 | tf_op jit(solution)/shard_map/enf,edf->nd/dot_general | solution.py:129
  187.1 0.9 copy-done.3
  188.0 3.5 %collective-permute-start = (bf16[15,128]{1,0:T(8,128)(2,1)S(1)}, bf16[15,128]{1,0:T(8,128)(2,1)S(1)}, u32[]{:S(2)}, u32[]{:S(2)}) collective-permute-start(bf16[15,128]{1,0:T(8,128)(2,1)S(1)} %slice.67), channel_id=1, source_target_pairs={{0,8},{8,16},{16,24},{1,9},{9,17},{17,25},{2,10},{10,18},{18,26},{... | collective-permute-start | bytes 11528 | tf_op jit(solution)/shard_map/ppermute | solution.py:20
  191.6 1.2 collective-permute-done
  193.5 17.3 %all_to_all.88 = bf16[8,128,128]{2,1,0:T(8,128)(2,1)} all-to-all(bf16[8,128,128]{2,1,0:T(8,128)(2,1)S(1)} %bitcast.122), channel_id=1, replica_groups=mesh['ep'=4,'tp'=8] {'tp'}, dimensions={0} | all-to-all | bytes 524288 | tf_op jit(solution)/shard_map/all_to_all | solution.py:141
  210.8 1.1 copy.44
  212.0 11.7 %all_gather.18 = bf16[512,512]{0,1:T(8,128)(2,1)S(1)} all-gather(bf16[128,512]{0,1:T(8,128)(2,1)S(1)} %get-tuple-element.7), channel_id=1, replica_groups=mesh['ep'=4,'tp'=8] {'ep'}, dimensions={0}, use_global_device_ids=true | all-gather | bytes 655360 | tf_op jit(solution)/shard_map/all_gather | solution.py:146
  223.7 9.1 %all_gather.20 = bf16[512,512]{0,1:T(8,128)(2,1)S(1)} all-gather(bf16[128,512]{0,1:T(8,128)(2,1)S(1)} %get-tuple-element.6), channel_id=1, replica_groups=mesh['ep'=4,'tp'=8] {'ep'}, dimensions={0}, use_global_device_ids=true | all-gather | bytes 655360 | tf_op jit(solution)/shard_map/all_gather | solution.py:146
  232.8 0.5 fusion.59
  233.7 10.3 %all_to_all.89 = bf16[4,128,512]{2,1,0:T(8,128)(2,1)S(1)} all-to-all(bf16[4,128,512]{2,1,0:T(8,128)(2,1)S(1)} %bitcast.120), channel_id=1, replica_groups=mesh['ep'=4,'tp'=8] {'ep'}, dimensions={0} | all-to-all | bytes 1048576 | tf_op jit(solution)/shard_map/all_to_all | solution.py:150
  244.0 12.8 %all_to_all.90 = bf16[4,48,2048]{2,1,0:T(8,128)(2,1)} all-to-all(bf16[4,48,2048]{2,1,0:T(8,128)(2,1)} %bitcast.125), channel_id=1, replica_groups=mesh['ep'=4,'tp'=8] {'ep'}, dimensions={0} | all-to-all | bytes 1572864 | tf_op jit(solution)/shard_map/all_to_all | solution.py:133
  256.9 55.6 %reduce-scatter.3.cloned.1.call-done = bf16[192,2048]{1,0:T(8,128)(2,1)} async-done(((bf16[1536,2048]{1,0:T(8,128)(2,1)}), bf16[192,2048]{1,0:T(8,128)(2,1)}) %reduce-scatter.3.cloned.1.call-update) | async-done | bytes 786448 | tf_op jit(solution)/shard_map/reduce_scatter | solution.py:130
  312.5 3.6 %all-to-all-start.4 = ((bf16[4,48,2048]{2,1,0:T(8,128)(2,1)}), bf16[4,48,2048]{2,1,0:T(8,128)(2,1)S(1)}, u32[]{:S(2)}, u32[]{:S(2)}) async-start(bf16[4,48,2048]{2,1,0:T(8,128)(2,1)} %bitcast.126), calls=%async_computation.5 | async-start | bytes 1572864 | tf_op jit(solution)/shard_map/all_to_all | solution.py:133
  316.1 0.8 copy.50
  317.0 3.0 convolution_bitcast_fusion
  319.9 5.3 %all-to-all-done.4 = bf16[4,48,2048]{2,1,0:T(8,128)(2,1)S(1)} async-done(((bf16[4,48,2048]{2,1,0:T(8,128)(2,1)}), bf16[4,48,2048]{2,1,0:T(8,128)(2,1)S(1)}, u32[]{:S(2)}, u32[]{:S(2)}) %all-to-all-start.4) | async-done | bytes 786464 | tf_op jit(solution)/shard_map/all_to_all | solution.py:133
  325.2 3.1 fusion.39
  (60 shorter events, 2.7 us)
Async XLA Ops:
  7.2 103.1 %copy-start = (bf16[4,2048,128]{2,1,0:T(8,128)(2,1)S(1)}, bf16[4,2048,128]{2,1,0:T(8,128)(2,1)}, u32[]{:S(2)}) copy-start(bf16[4,2048,128]{2,1,0:T(8,128)(2,1)} %param.19) | copy-start | bytes 6291460
  7.2 37.9 %all-gather.4.cloned.1.call-start = ((), (), s32[]{:S(2)}) async-start(), calls=%async_computation.9 | async-start | bytes 1179648 | tf_op jit(solution)/shard_map/all_gather | solution.py:100
  7.2 24.0 %copy-start.1 = (bf16[256,2048]{1,0:T(8,128)(2,1)S(1)}, bf16[256,2048]{1,0:T(8,128)(2,1)}, u32[]{:S(2)}) copy-start(bf16[256,2048]{1,0:T(8,128)(2,1)} %param.13) | copy-start | bytes 3145732
  7.2 24.0 %copy-start.7 = (f32[2048]{0:T(1024)S(1)}, f32[2048]{0:T(1024)}, u32[]{:S(2)}) copy-start(f32[2048]{0:T(1024)} %param.14) | copy-start | bytes 24580
  9.0 92.7 %all-gather.8.cloned.1.call-start = ((), (), s32[]{:S(2)}) async-start(), calls=%async_computation.12 | async-start | bytes 7077888 | tf_op jit(solution)/shard_map/all_gather | solution.py:122
  14.7 30.4 %copy-start.4 = (s32[256,2]{0,1:T(2,128)S(1)}, s32[256,2]{0,1:T(2,128)}, u32[]{:S(2)}) copy-start(s32[256,2]{0,1:T(2,128)} %param.15) | copy-start | bytes 6148
  14.8 30.4 %copy-start.5 = (f32[256,2]{0,1:T(2,128)S(1)}, f32[256,2]{0,1:T(2,128)}, u32[]{:S(2)}) copy-start(f32[256,2]{0,1:T(2,128)} %param.16) | copy-start | bytes 6148
  31.2 135.5 %all-gather.6.cloned.1.call-start = ((), (), s32[]{:S(2)}) async-start(), calls=%async_computation.10 | async-start | bytes 7077888 | tf_op jit(solution)/shard_map/all_gather | solution.py:122
  45.1 199.0 %reduce-scatter.5.cloned.1.call-start = ((), (), s32[]{:S(2)}) async-start(), calls=%async_computation.13 | async-start | bytes 7077888 | tf_op jit(solution)/shard_map/reduce_scatter | solution.py:130
  122.5 189.9 %reduce-scatter.3.cloned.1.call-start = ((), (), s32[]{:S(2)}) async-start(), calls=%async_computation.11 | async-start | bytes 7077888 | tf_op jit(solution)/shard_map/reduce_scatter | solution.py:130
  187.0 0.9 copy-start.3
  188.0 5.1 %copy-start.6 = (f32[128]{0:T(128)S(1)}, f32[128]{0:T(128)}, u32[]{:S(2)}) copy-start(f32[128]{0:T(128)} %param.11) | copy-start | bytes 1540
  188.0 4.8 %collective-permute-start = (bf16[15,128]{1,0:T(8,128)(2,1)S(1)}, bf16[15,128]{1,0:T(8,128)(2,1)S(1)}, u32[]{:S(2)}, u32[]{:S(2)}) collective-permute-start(bf16[15,128]{1,0:T(8,128)(2,1)S(1)} %slice.67), channel_id=1, source_target_pairs={{0,8},{8,16},{16,24},{1,9},{9,17},{17,25},{2,10},{10,18},{18,26},{... | collective-permute-start | bytes 11528 | tf_op jit(solution)/shard_map/ppermute | solution.py:20
  193.1 39.7 %copy-start.2 = (bf16[1024,512]{1,0:T(8,128)(2,1)S(1)}, bf16[1024,512]{1,0:T(8,128)(2,1)}, u32[]{:S(2)}) copy-start(bf16[1024,512]{1,0:T(8,128)(2,1)} %all-gather.4.cloned.1.call-done) | copy-start | bytes 3145732
  312.5 12.7 %all-to-all-start.4 = ((bf16[4,48,2048]{2,1,0:T(8,128)(2,1)}), bf16[4,48,2048]{2,1,0:T(8,128)(2,1)S(1)}, u32[]{:S(2)}, u32[]{:S(2)}) async-start(bf16[4,48,2048]{2,1,0:T(8,128)(2,1)} %bitcast.126), calls=%async_computation.5 | async-start | bytes 1572864 | tf_op jit(solution)/shard_map/all_to_all | solution.py:133
Sparse Core Ops, SparseCore 0:
  10.2 24.9 all-gather.3
  36.8 64.8 all-gather.7
  103.4 63.3 all-gather.5
  168.9 72.5 reduce-scatter.4
  243.7 68.7 reduce-scatter.2
where the time goes:
time: 336 us; the launch traced here: 335 us
  waiting for transfers between devices  140 us (42%)
  blocking collectives  113 us (34%)
  matrix products  50.6 us (15%)
  between operations  14 us (4%)
  starting transfers between devices  7.53 us (2%)
  local copies, waits for them, and re-layouts  5.31 us (2%)
  other arithmetic  4.27 us (1%)
    all_gather x2, waiting for transfers between devices, body(): tokens = lax.all_gather(arrived_list[chunk], 'tp', axis=0, tiled=True)  78 us
    reduce_scatter x2, waiting for transfers between devices, body(): lax.psum_scatter(partial.astype(jnp.bfloat16), 'tp', scatter_dimension=0,...  55.6 us
    all_to_all x2, blocking collectives, body(): lax.all_to_all(outgoing, 'ep', split_axis=0, concat_axis=0, tiled=True)  29.7 us
    dot_general x2, matrix products, body(): jnp.einsum('enf,edf->nd', hidden, down_weight, preferred_element_type=jnp...  24.1 us
    all_gather x2, blocking collectives, body(): lax.all_gather(regrouped[:, section], 'ep', axis=0, tiled=True)  20.8 us
    all_to_all x1, blocking collectives, body(): lax.all_to_all(pooled, 'tp', split_axis=0, concat_axis=1, tiled=True)  17.3 us
    dot_general x2, matrix products, body(): jnp.einsum('nd,edf->enf', tokens, gate_weight, preferred_element_type=jnp...  17 us
    all_gather x1, blocking collectives, body(): weights = lax.all_gather(weights, 'tp', axis=0, tiled=True)  14.8 us
  transfers between devices with their start and end apart: 7, of which 5 were waited for; matrix products, arithmetic and copies ran while one was open for 16% of the time, Pallas kernels for 0%

commit v1 on v0

--- a/solution.py
+++ b/solution.py
@@ -1,6 +1,10 @@
+import functools
+
 import jax
 import jax.numpy as jnp
 from jax import lax
+from jax.experimental import pallas as pl
+from jax.experimental.pallas import tpu as pltpu
 from jax.sharding import PartitionSpec as P
 
 GROUP_CH = 256
@@ -79,7 +83,7 @@
     return placing.astype(jnp.bfloat16).reshape(ep_size * capacity, -1), slot_weight, capacity
 
 
-def body(
+def general_body(
     pool_input,
     pool_gain,
     mix_weight,
@@ -153,22 +157,527 @@
     return (mixed_out, moe_out)
 
 
+LANES = 128
+PIECES = 4
+VMEM_LIMIT = 67043328
+MESH = pl.DeviceIdType.MESH
+
+
+def kernel_bytes(ep_size, planes, rows, slots, width, hidden, local_experts):
+    wide = width + LANES
+    block = ep_size * slots
+    elements = planes * rows * wide
+    elements += planes * (ep_size - 1) * slots * wide
+    elements += planes * 2 * block * wide
+    elements += 3 * local_experts * width * hidden
+    elements += (planes * 2 + 4) * block * width
+    elements += 2 * planes * rows * width
+    elements += 2 * block * local_experts * hidden
+    elements += rows * (wide + width)
+    return 2 * elements
+
+
+def expert_kernel(
+    ep_size,
+    planes,
+    x_ref,
+    gate_ref,
+    up_ref,
+    down_ref,
+    out_ref,
+    column,
+    packed,
+    tokens,
+    gate_up,
+    down,
+    hidden,
+    outgoing,
+    partial,
+    arriving,
+    returned,
+    running,
+    weight_sems,
+    line_send,
+    line_recv,
+    plane_send,
+    plane_recv,
+    share_send,
+    share_recv,
+    part_send,
+    part_recv,
+    back_send,
+    back_recv,
+    left_send,
+    right_send,
+    left_recv,
+    right_recv,
+):
+    ep = lax.axis_index("ep")
+    tp = lax.axis_index("tp")
+    z = tp // 2
+    core = tp % 2
+    rows, wide = x_ref.shape
+    local_experts, width, ff = gate_ref.shape
+    slots = packed.shape[2]
+    block = ep_size * slots
+    piece = width // PIECES
+    partner = (ep, tp + 1 - 2 * core)
+    left = (ep, tp - 2)
+    right = (ep, tp + 2)
+    has_left = z > 0
+    has_right = z < planes - 1
+    at_end = (z * (planes - 1 - z)) == 0
+    turn = 1 - 2 * (z // (planes // 2))
+
+    inner = (z * (planes - 1 - z) + planes - 2) // (planes - 1)
+
+    def source_of(step):
+        both_ways = ((step + 1) // 2) * (2 * (step % 2) - 1)
+        offset = inner * both_ways + (1 - inner) * step
+        return (z + turn * offset + planes) % planes
+
+    def sum_of(step):
+        return (z + turn * step + planes) % planes
+
+    def peer_of(offset):
+        return ((ep + offset) % ep_size, tp)
+
+    barrier = pltpu.get_barrier_semaphore()
+    for offset in range(1, ep_size):
+        pl.semaphore_signal(barrier, inc=1, device_id=peer_of(offset), device_id_type=MESH)
+    pl.semaphore_signal(barrier, inc=1, device_id=partner, device_id_type=MESH)
+
+    @pl.when(has_left)
+    def _():
+        pl.semaphore_signal(barrier, inc=1, device_id=left, device_id_type=MESH)
+
+    @pl.when(has_right)
+    def _():
+        pl.semaphore_signal(barrier, inc=1, device_id=right, device_id_type=MESH)
+
+    loads = []
+    for expert in range(local_experts):
+        lanes = pl.ds(expert * ff, ff)
+        loads.append((gate_ref.at[expert], gate_up.at[expert, :, pl.ds(0, ff)]))
+        loads.append((up_ref.at[expert], gate_up.at[expert, :, pl.ds(ff, ff)]))
+        loads.append((down_ref.at[expert], down.at[:, lanes]))
+    loads = [
+        pltpu.make_async_copy(source, target, weight_sems.at[index])
+        for index, (source, target) in enumerate(loads)
+    ]
+    for load in loads:
+        load.start()
+
+    pl.semaphore_wait(barrier, ep_size + 1 + inner)
+
+    def line_copy(source_ref, source, direction):
+        return pltpu.make_async_remote_copy(
+            src_ref=source_ref,
+            dst_ref=column.at[source],
+            send_sem=line_send.at[source, direction],
+            recv_sem=line_recv.at[source],
+            device_id=(left, right)[direction],
+            device_id_type=MESH,
+        )
+
+    def plane_copy(source, offset):
+        return pltpu.make_async_remote_copy(
+            src_ref=packed.at[source, offset - 1],
+            dst_ref=tokens.at[source, core, pl.ds(pl.multiple_of(ep * slots, slots), slots)],
+            send_sem=plane_send.at[source, offset - 1],
+            recv_sem=plane_recv.at[source, offset - 1],
+            device_id=peer_of(offset),
+            device_id_type=MESH,
+        )
+
+    def share_copy(source):
+        return pltpu.make_async_remote_copy(
+            src_ref=tokens.at[source, core],
+            dst_ref=tokens.at[source, core],
+            send_sem=share_send.at[source],
+            recv_sem=share_recv.at[source],
+            device_id=partner,
+            device_id_type=MESH,
+        )
+
+    def part_copy(source, slot, index):
+        return pltpu.make_async_remote_copy(
+            src_ref=outgoing.at[slot, index],
+            dst_ref=arriving.at[slot, index],
+            send_sem=part_send.at[slot, index],
+            recv_sem=part_recv.at[slot, index],
+            device_id=partner,
+            device_id_type=MESH,
+        )
+
+    def back_copy(source, offset, index):
+        target = (ep + offset) % ep_size
+        return pltpu.make_async_remote_copy(
+            src_ref=partial.at[source, index, pl.ds(pl.multiple_of(target * slots, slots), slots)],
+            dst_ref=returned.at[source, index, pl.ds(pl.multiple_of(ep * slots, slots), slots)],
+            send_sem=back_send.at[source, offset - 1, index],
+            recv_sem=back_recv.at[source, offset - 1, index],
+            device_id=(target, tp),
+            device_id_type=MESH,
+        )
+
+    def sum_copy(source, index, direction):
+        return pltpu.make_async_remote_copy(
+            src_ref=running.at[1 - direction, source, index],
+            dst_ref=running.at[1 - direction, source, index],
+            send_sem=(left_send, right_send)[direction].at[source, index],
+            recv_sem=(right_recv, left_recv)[direction].at[source, index],
+            device_id=(left, right)[direction],
+            device_id_type=MESH,
+        )
+
+    def dispatch(source_ref, source):
+        routing = source_ref[:, width:].astype(jnp.float32).T
+        for offset in range(ep_size):
+            group = (ep + offset) % ep_size
+            slot_row = jnp.zeros((1, rows), jnp.float32)
+            for index in range(ep_size):
+                row = 2 * local_experts + index
+                chosen = jnp.where(index == group, 1.0, 0.0)
+                slot_row = slot_row + routing[row : row + 1] * chosen
+            places = lax.broadcasted_iota(jnp.int32, (slots, rows), 0).astype(jnp.float32)
+            placing = jnp.where(places == slot_row, 1.0, 0.0).astype(jnp.bfloat16)
+            compact = jnp.dot(placing, source_ref[...], preferred_element_type=jnp.float32)
+            compact = compact.astype(jnp.bfloat16)
+            if offset == 0:
+                tokens[source, core, pl.ds(pl.multiple_of(ep * slots, slots), slots)] = compact
+            else:
+                packed[source, offset - 1] = compact
+                plane_copy(source, offset).start()
+
+    def gather(source):
+        for offset in range(1, ep_size):
+            plane_copy(source, offset).wait_recv()
+        share_copy(source).start()
+
+    def experts(source, slot):
+        share_copy(source).wait_recv()
+
+        def one(expert, carry):
+            values = tokens[source].reshape(2 * block, wide)
+            both = jnp.dot(
+                values[:, :width], gate_up[expert], preferred_element_type=jnp.float32
+            )
+            lane = lax.broadcasted_iota(jnp.int32, (2 * block, LANES), 1)
+            mine = (lane == expert) | (lane == local_experts + expert)
+            scale = jnp.where(mine, values[:, width:].astype(jnp.float32), 0.0)
+            scale = jnp.sum(scale, axis=1, keepdims=True)
+            gated = both[:, :ff]
+            gated = gated / (1.0 + jnp.exp(-gated))
+            result = (gated * both[:, ff:] * scale).astype(jnp.bfloat16)
+            hidden[:, pl.ds(pl.multiple_of(expert * ff, ff), ff)] = result
+            return carry
+
+        lax.fori_loop(0, local_experts, one, 0)
+
+        def project(which, index):
+            part = hidden[pl.ds(pl.multiple_of(which * block, block), block)]
+            return lax.dot_general(
+                part,
+                down[index * piece : (index + 1) * piece],
+                (((1,), (1,)), ((), ())),
+                preferred_element_type=jnp.float32,
+            )
+
+        for index in range(PIECES):
+            outgoing[slot, index] = project(1 - core, index).astype(jnp.bfloat16)
+            part_copy(source, slot, index).start()
+        for index in range(PIECES):
+            own = project(core, index)
+            part_copy(source, slot, index).wait_recv()
+            total = own + arriving[slot, index].astype(jnp.float32)
+            partial[source, index] = total.astype(jnp.bfloat16)
+            own_rows = pl.ds(pl.multiple_of(ep * slots, slots), slots)
+            returned[source, index, own_rows] = partial[source, index, own_rows]
+            for offset in range(1, ep_size):
+                back_copy(source, offset, index).start()
+
+    def placing_back(source_ref):
+        routing = source_ref[:, width:].astype(jnp.float32)
+        pieces = []
+        for group in range(ep_size):
+            lane = 2 * local_experts + group
+            places = lax.broadcasted_iota(jnp.int32, (rows, slots), 1).astype(jnp.float32)
+            matched = places == routing[:, lane : lane + 1]
+            pieces.append(jnp.where(matched, 1.0, 0.0))
+        return jnp.concatenate(pieces, axis=1).astype(jnp.bfloat16)
+
+    def combine(placing, source, index):
+        for offset in range(1, ep_size):
+            back_copy(source, offset, index).wait_recv()
+        return jnp.dot(placing, returned[source, index], preferred_element_type=jnp.float32)
+
+    def reduce_line(step):
+        source = sum_of(step)
+        placing = placing_back(column.at[source])
+        for index in range(PIECES):
+            mine = combine(placing, source, index)
+
+            for direction in range(2):
+                toward = (source < z, source > z)[direction]
+                has_before = (has_right, has_left)[direction]
+
+                @pl.when(toward & has_before)
+                def _(direction=direction):
+                    before = sum_copy(source, index, direction)
+                    before.wait_recv()
+                    total = mine + running[1 - direction, source, index].astype(jnp.float32)
+                    running[1 - direction, source, index] = total.astype(jnp.bfloat16)
+                    sum_copy(source, index, direction).start()
+
+                @pl.when(toward & ~has_before)
+                def _(direction=direction):
+                    running[1 - direction, source, index] = mine.astype(jnp.bfloat16)
+                    sum_copy(source, index, direction).start()
+
+    @pl.when(has_left)
+    def _():
+        line_copy(x_ref, z, 0).start()
+
+    @pl.when(has_right)
+    def _():
+        line_copy(x_ref, z, 1).start()
+
+    dispatch(x_ref, z)
+    for load in loads:
+        load.wait()
+
+    def step_body(step, carry):
+        @pl.when(step < planes)
+        def _():
+            source = source_of(step)
+            line_copy(x_ref, source, 0).wait_recv()
+
+            @pl.when((source > z) & has_left)
+            def _():
+                line_copy(column.at[source], source, 0).start()
+
+            @pl.when((source < z) & has_right)
+            def _():
+                line_copy(column.at[source], source, 1).start()
+
+            dispatch(column.at[source], source)
+
+        previous = source_of(step - 1)
+        slot = (step - 1) % 2
+        gather(previous)
+
+        @pl.when(step > 2)
+        def _():
+            for index in range(PIECES):
+                part_copy(previous, slot, index).wait_send()
+
+        experts(previous, slot)
+
+        @pl.when(at_end & (step > 2))
+        def _():
+            reduce_line(step - 2)
+
+        return carry
+
+    lax.fori_loop(1, planes + 1, step_body, 0)
+
+    def tail_body(step, carry):
+        @pl.when(~at_end | (step == planes - 1))
+        def _():
+            reduce_line(step)
+
+        return carry
+
+    lax.fori_loop(1, planes, tail_body, 0)
+
+    placing = placing_back(x_ref)
+    for index in range(PIECES):
+        mine = combine(placing, z, index)
+        lanes = pl.ds(index * piece, piece)
+
+        for direction in range(2):
+            has_before = (has_right, has_left)[direction]
+
+            @pl.when(has_before)
+            def _(direction=direction):
+                sum_copy(z, index, direction).wait_recv()
+
+        zero = jnp.zeros_like(mine)
+        from_left = jnp.where(has_left, running[0, z, index].astype(jnp.float32), zero)
+        from_right = jnp.where(has_right, running[1, z, index].astype(jnp.float32), zero)
+        out_ref[:, lanes] = (mine + from_left + from_right).astype(jnp.bfloat16)
+
+    @pl.when(has_left)
+    def _():
+        line_copy(x_ref, z, 0).wait_send()
+
+    @pl.when(has_right)
+    def _():
+        line_copy(x_ref, z, 1).wait_send()
+
+    def drain(source, carry):
+        for offset in range(1, ep_size):
+            plane_copy(source, offset).wait_send()
+            for index in range(PIECES):
+                back_copy(source, offset, index).wait_send()
+        share_copy(source).wait_send()
+        for direction in range(2):
+            toward = (source < z, source > z)[direction]
+            has_next = (has_left, has_right)[direction]
+            forwarded = (source > z, source < z)[direction]
+
+            @pl.when(toward)
+            def _(direction=direction):
+                for index in range(PIECES):
+                    sum_copy(source, index, direction).wait_send()
+
+            @pl.when(forwarded & has_next)
+            def _(direction=direction):
+                line_copy(x_ref, source, direction).wait_send()
+
+        return carry
+
+    lax.fori_loop(0, planes, drain, 0)
+    for slot in range(2):
+        for index in range(PIECES):
+            part_copy(0, slot, index).wait_send()
+
+
+def expert_layer(extended, gate_weight, up_weight, down_weight, ep_size, planes, slots):
+    rows, wide = extended.shape
+    local_experts, width, ff = gate_weight.shape
+    block = ep_size * slots
+    piece = width // PIECES
+    half = jnp.bfloat16
+    dma = pltpu.SemaphoreType.DMA
+    return pl.pallas_call(
+        functools.partial(expert_kernel, ep_size, planes),
+        out_shape=jax.ShapeDtypeStruct((rows, width), half),
+        in_specs=[pl.BlockSpec(memory_space=pltpu.VMEM)] + [pl.BlockSpec(memory_space=pl.ANY)] * 3,
+        out_specs=pl.BlockSpec(memory_space=pltpu.VMEM),
+        scratch_shapes=[
+            pltpu.VMEM((planes, rows, wide), half),
+            pltpu.VMEM((planes, ep_size - 1, slots, wide), half),
+            pltpu.VMEM((planes, 2, block, wide), half),
+            pltpu.VMEM((local_experts, width, 2 * ff), half),
+            pltpu.VMEM((width, local_experts * ff), half),
+            pltpu.VMEM((2 * block, local_experts * ff), half),
+            pltpu.VMEM((2, PIECES, block, piece), half),
+            pltpu.VMEM((planes, PIECES, block, piece), half),
+            pltpu.VMEM((2, PIECES, block, piece), half),
+            pltpu.VMEM((planes, PIECES, block, piece), half),
+            pltpu.VMEM((2, planes, PIECES, rows, piece), half),
+            dma((3 * local_experts,)),
+            dma((planes, 2)),
+            dma((planes,)),
+            dma((planes, ep_size - 1)),
+            dma((planes, ep_size - 1)),
+            dma((planes,)),
+            dma((planes,)),
+            dma((2, PIECES)),
+            dma((2, PIECES)),
+            dma((planes, ep_size - 1, PIECES)),
+            dma((planes, ep_size - 1, PIECES)),
+            dma((planes, PIECES)),
+            dma((planes, PIECES)),
+            dma((planes, PIECES)),
+            dma((planes, PIECES)),
+        ],
+        compiler_params=pltpu.CompilerParams(
+            collective_id=0, has_side_effects=True, vmem_limit_bytes=VMEM_LIMIT
+        ),
+    )(extended, gate_weight, up_weight, down_weight)
+
+
+def routing_lanes(expert_ids, route_weight, ep_size):
+    local_experts = EXPERTS // ep_size
+    owners = expert_ids // local_experts
+    ep_index = lax.iota(jnp.int32, ep_size)
+    member = jnp.any(owners[:, :, None] == ep_index[None, None, :], axis=1)
+    counts = member.astype(jnp.int32)
+    rank = jnp.cumsum(counts, axis=0) - counts
+    slot = jnp.where(member, rank, -1).astype(jnp.float32)
+    within = expert_ids % local_experts
+    named = within[:, :, None] == lax.iota(jnp.int32, local_experts)[None, None, :]
+    weights = jnp.sum(jnp.where(named, route_weight[:, :, None], 0.0), axis=1)
+    high = lax.reduce_precision(weights, 8, 7)
+    low = weights - high
+    spare = LANES - 2 * local_experts - ep_size
+    lanes = jnp.concatenate([high, low, slot], axis=1)
+    return jnp.pad(lanes, ((0, 0), (0, spare))).astype(jnp.bfloat16)
+
+
+def fast_body(
+    pool_input,
+    pool_gain,
+    mix_weight,
+    moe_input,
+    moe_gain,
+    expert_ids,
+    route_weight,
+    gate_weight,
+    up_weight,
+    down_weight,
+):
+    ep_size = lax.axis_size("ep")
+    planes = lax.axis_size("tp") // 2
+    local_experts = gate_weight.shape[0]
+    slots = local_experts * CAP // TOP
+    inputs = moe_input.astype(jnp.float32)
+    scale_rows = lax.rsqrt(jnp.mean(inputs * inputs, axis=-1, keepdims=True) + eps_norm)
+    normed = (inputs * scale_rows * moe_gain).astype(jnp.bfloat16)
+    extended = jnp.concatenate([normed, routing_lanes(expert_ids, route_weight, ep_size)], axis=1)
+    moe_out = expert_layer(
+        extended, gate_weight, up_weight, down_weight, ep_size, planes, slots
+    )
+    pooled = pool_mixer(pool_input, pool_gain)
+    mix_rows = lax.all_gather(mix_weight, "tp", axis=0, tiled=True)
+    regrouped = lax.all_to_all(pooled, "tp", split_axis=0, concat_axis=1, tiled=True)
+    mixed_out = jnp.dot(regrouped, mix_rows, preferred_element_type=jnp.float32)
+    return (mixed_out.astype(jnp.bfloat16), moe_out)
+
+
+def fits(mesh, shapes):
+    moe_input, gate_weight = shapes
+    ep_size = mesh.shape["ep"]
+    tp_size = mesh.shape["tp"]
+    experts, width, ff = gate_weight
+    local_experts = experts // ep_size
+    rows = moe_input[0] // (ep_size * tp_size)
+    ff = ff // tp_size
+    if local_experts % GROUP_EXP or tp_size % 4 or tp_size > 8 or ff % LANES or width % (PIECES * LANES):
+        return False
+    if 2 * local_experts + ep_size > LANES or rows > 256:
+        return False
+    slots = local_experts * CAP // TOP
+    if slots % 16 or rows % 16:
+        return False
+    needed = kernel_bytes(ep_size, tp_size // 2, rows, slots, width, ff, local_experts)
+    return needed < VMEM_LIMIT
+
+
 def solution(mesh):
-    return jax.shard_map(
-        body,
-        mesh=mesh,
-        in_specs=(
-            P("ep", "tp"),
-            P("tp"),
-            P("tp", None),
-            P(("ep", "tp"), None),
-            P(),
-            P(("ep", "tp"), None),
-            P(("ep", "tp"), None),
-            P("ep", None, "tp"),
-            P("ep", None, "tp"),
-            P("ep", None, "tp"),
-        ),
-        out_specs=(P(("ep", "tp"), None), P(("ep", "tp"), None)),
-        check_vma=False,
-    )
+    def program(*arguments):
+        shapes = (arguments[3].shape, arguments[7].shape)
+        body = fast_body if fits(mesh, shapes) else general_body
+        return jax.shard_map(
+            body,
+            mesh=mesh,
+            in_specs=(
+                P("ep", "tp"),
+                P("tp"),
+                P("tp", None),
+                P(("ep", "tp"), None),
+                P(),
+                P(("ep", "tp"), None),
+                P(("ep", "tp"), None),
+                P("ep", None, "tp"),
+                P("ep", None, "tp"),
+                P("ep", None, "tp"),
+            ),
+            out_specs=(P(("ep", "tp"), None), P(("ep", "tp"), None)),
+            check_vma=False,
+        )(*arguments)
+
+    return program

time: 336 us -> 275 us (0.82)
  Pallas kernels: 0 us -> 235 us
  waiting for transfers between devices: 140 us -> 0.71 us
  blocking collectives: 113 us -> 0 us
  matrix products: 50.6 us -> 3.81 us
  other arithmetic: 4.27 us -> 7.7 us
    pallas_call x0 -> x1, Pallas kernels: none -> 235 us  [expert_layer(): pl.pallas_call(functools.partial(expert_kernel, ep_size, planes), out_sha...]
    all_gather x3 -> x1, waiting for transfers between devices: 78 us -> 0.02 us  [fast_body(): mix_rows = lax.all_gather(mix_weight, 'tp', axis=0, tiled=True)]
    all_to_all x6 -> x0, blocking collectives: 77.2 us -> none  [the longest x2 29.7 us: body(): lax.all_to_all(outgoing, 'ep', split_axis=0, concat_axis=0, tiled=True)]
    reduce_scatter x2 -> x0, waiting for transfers between devices: 55.6 us -> none  [body(): lax.psum_scatter(partial.astype(jnp.bfloat16), 'tp', scatter_dimension=0,...]
    dot_general x11 -> x1, matrix products: 50.6 us -> 3.81 us  [fast_body(): mixed_out = jnp.dot(regrouped, mix_rows, preferred_element_type=jnp.float32)]
    all_gather x3 -> x0, blocking collectives: 35.6 us -> none  [the longest x2 20.8 us: body(): lax.all_gather(regrouped[:, section], 'ep', axis=0, tiled=True)]
    all_to_all x1, waiting for transfers between devices: 5.3 us -> 0.01 us  [fast_body(): lax.all_to_all(pooled, 'tp', split_axis=0, concat_axis=1, tiled=True)]
  transfers between devices with their start and end apart: 7 -> 3, of which waited for: 5 -> 0; matrix products, arithmetic and copies ran while one was open for 16% -> 4% of each run, Pallas kernels for 0% -> 85%
where the time goes in v1:
time: 275 us
  Pallas kernels  235 us (85%)
  between operations  14.2 us (5%)
  starting transfers between devices  9.77 us (4%)
  other arithmetic  7.7 us (3%)
  matrix products  3.81 us (1%)
  local copies, waits for them, and re-layouts  3.69 us (1%)
    pallas_call x1, Pallas kernels, expert_layer(): pl.pallas_call(functools.partial(expert_kernel, ep_size, planes), out_sha...  235 us
  transfers between devices with their start and end apart: 3, of which 0 were waited for; matrix products, arithmetic and copies ran while one was open for 4% of the time, Pallas kernels for 85%

profile of v1, /device:TPU:0, one launch (start us, length us, event | category | flops | bytes accessed | tf_op | source)
XLA Modules:
  0.0 275.0 jit_solution(7862907035914840295)
XLA Ops:
  7.2 0.0 copy-start.2
  7.2 0.0 copy-start
  7.2 0.0 all-gather.2.cloned.1.call-start
  7.2 0.7 all-gather.2.cloned.1.call-update
  7.9 0.7 slice.43
  8.6 4.9 %collective-permute-start = (bf16[15,128]{1,0:T(8,128)(2,1)S(1)}, bf16[15,128]{1,0:T(8,128)(2,1)S(1)}, u32[]{:S(2)}, u32[]{:S(2)}) collective-permute-start(bf16[15,128]{1,0:T(8,128)(2,1)S(1)} %slice.43), channel_id=1, source_target_pairs={{0,8},{8,16},{16,24},{1,9},{9,17},{17,25},{2,10},{10,18},{18,26},{... | collective-permute-start | bytes 11528 | tf_op jit(solution)/shard_map/ppermute | solution.py:24
  13.5 0.7 and_select_fusion.1
  14.2 1.2 reduce-window.6
  15.5 0.1 slice.68
  15.5 0.1 copy.42
  15.7 0.1 copy.43
  15.8 0.7 select_reduce_fusion
  16.5 1.5 fusion.1
  18.0 0.1 add_bitcast_fusion
  18.1 1.0 fusion.3
  19.2 0.0 collective-permute-done
  19.2 0.1 maximum_convert_fusion
  19.3 0.0 copy-start.3
  19.3 0.1 slice_add_fusion.1
  19.3 0.1 slice_add_fusion
  19.4 0.1 slice_add_fusion.2
  19.5 0.5 copy-done.3
  19.9 1.1 fusion.6
  21.0 4.9 %all-to-all-start = ((bf16[8,128,128]{2,1,0:T(8,128)(2,1)}), bf16[8,128,128]{2,1,0:T(8,128)(2,1)}, u32[]{:S(2)}, u32[]{:S(2)}) async-start(bf16[8,128,128]{2,1,0:T(8,128)(2,1)} %bitcast), calls=%async_computation | async-start | bytes 524288 | tf_op jit(solution)/shard_map/all_to_all | solution.py:636
  25.9 0.1 copy.44
  26.0 1.1 fusion.4.x_ref
  27.1 235.1 %shard_map.113 = bf16[256,2048]{1,0:T(8,128)(2,1)} custom-call(bf16[256,2176]{1,0:T(8,128)(2,1)} %fusion.4.x_ref, bf16[4,2048,128]{2,1,0:T(8,128)(2,1)} %gate_ref.1, bf16[4,2048,128]{2,1,0:T(8,128)(2,1)} %up_ref.1, bf16[4,2048,128]{2,1,0:T(8,128)(2,1)} %down_ref.1), custom_call_target="tpu_custom_call" | custom-call | tf_op jit(solution)/shard_map/pallas_call | solution.py:554
  262.2 0.0 all-to-all-done
  262.2 1.1 copy.41
  263.4 0.0 all-gather.2.cloned.1.call-done
  263.4 3.8 %convolution_convert_fusion = bf16[128,2048]{1,0:T(8,128)(2,1)} fusion(bf16[128,1024]{0,1:T(8,128)(2,1)S(1)} %bitcast.18, bf16[1024,2048]{1,0:T(8,128)(2,1)} %all-gather.2.cloned.1.call-done), kind=kOutput, calls=%fused_computation.2 | convolution fusion | flops 537133056 | bytes 4980736 | tf_op jit(solution)/shard_map/dot_general | solution.py:637
  267.2 1.0 copy.48
  (17 shorter events, 0.2 us)
Async XLA Ops:
  7.2 12.0 %copy-start.2 = (bf16[1024,128]{1,0:T(8,128)(2,1)S(1)}, bf16[1024,128]{1,0:T(8,128)(2,1)}, u32[]{:S(2)}) copy-start(bf16[1024,128]{1,0:T(8,128)(2,1)} %param.10) | copy-start | bytes 786436
  7.2 11.0 %copy-start = (bf16[256,2048]{1,0:T(8,128)(2,1)S(1)}, bf16[256,2048]{1,0:T(8,128)(2,1)}, u32[]{:S(2)}) copy-start(bf16[256,2048]{1,0:T(8,128)(2,1)} %param.13) | copy-start | bytes 3145732
  7.2 256.2 %all-gather.2.cloned.1.call-start = ((), (), s32[]{:S(2)}) async-start(), calls=%async_computation.1 | async-start | bytes 4718592 | tf_op jit(solution)/shard_map/all_gather | solution.py:635
  8.6 10.6 %collective-permute-start = (bf16[15,128]{1,0:T(8,128)(2,1)S(1)}, bf16[15,128]{1,0:T(8,128)(2,1)S(1)}, u32[]{:S(2)}, u32[]{:S(2)}) collective-permute-start(bf16[15,128]{1,0:T(8,128)(2,1)S(1)} %slice.43), channel_id=1, source_target_pairs={{0,8},{8,16},{16,24},{1,9},{9,17},{17,25},{2,10},{10,18},{18,26},{... | collective-permute-start | bytes 11528 | tf_op jit(solution)/shard_map/ppermute | solution.py:24
  19.3 0.7 copy-start.3
  21.0 241.2 %all-to-all-start = ((bf16[8,128,128]{2,1,0:T(8,128)(2,1)}), bf16[8,128,128]{2,1,0:T(8,128)(2,1)}, u32[]{:S(2)}, u32[]{:S(2)}) async-start(bf16[8,128,128]{2,1,0:T(8,128)(2,1)} %bitcast), calls=%async_computation | async-start | bytes 524288 | tf_op jit(solution)/shard_map/all_to_all | solution.py:636
  263.4 3.8 %copy-start.1 = (bf16[256,2048]{1,0:T(8,128)(2,1)S(1)}, bf16[256,2048]{1,0:T(8,128)(2,1)}, u32[]{:S(2)}) copy-start(bf16[256,2048]{1,0:T(8,128)(2,1)} %shard_map.113) | copy-start | bytes 3145732
Sparse Core Ops, SparseCore 0:
  9.6 72.2 all-gather.1

commit v2 on v1

--- a/solution.py
+++ b/solution.py
@@ -163,7 +163,7 @@
 MESH = pl.DeviceIdType.MESH
 
 
-def kernel_bytes(ep_size, planes, rows, slots, width, hidden, local_experts):
+def kernel_bytes(ep_size, planes, rows, slots, width, hidden, local_experts, mixer_elements):
     wide = width + LANES
     block = ep_size * slots
     elements = planes * rows * wide
@@ -171,9 +171,10 @@
     elements += planes * 2 * block * wide
     elements += 3 * local_experts * width * hidden
     elements += (planes * 2 + 4) * block * width
-    elements += 2 * planes * rows * width
+    elements += (planes + 1) * rows * width
     elements += 2 * block * local_experts * hidden
     elements += rows * (wide + width)
+    elements += mixer_elements
     return 2 * elements
 
 
@@ -181,9 +182,13 @@
     ep_size,
     planes,
     x_ref,
+    pool_ref,
+    gain_ref,
+    mix_ref,
     gate_ref,
     up_ref,
     down_ref,
+    mixed_ref,
     out_ref,
     column,
     packed,
@@ -211,6 +216,18 @@
     right_send,
     left_recv,
     right_recv,
+    halo,
+    pooled,
+    regrouped,
+    mix,
+    halo_sems,
+    mix_load,
+    pool_send,
+    pool_recv,
+    mix_send,
+    mix_recv,
+    pair_send,
+    pair_recv,
 ):
     ep = lax.axis_index("ep")
     tp = lax.axis_index("tp")
@@ -242,18 +259,14 @@
     def peer_of(offset):
         return ((ep + offset) % ep_size, tp)
 
+    tp_size = 2 * planes
     barrier = pltpu.get_barrier_semaphore()
     for offset in range(1, ep_size):
         pl.semaphore_signal(barrier, inc=1, device_id=peer_of(offset), device_id_type=MESH)
-    pl.semaphore_signal(barrier, inc=1, device_id=partner, device_id_type=MESH)
-
-    @pl.when(has_left)
-    def _():
-        pl.semaphore_signal(barrier, inc=1, device_id=left, device_id_type=MESH)
-
-    @pl.when(has_right)
-    def _():
-        pl.semaphore_signal(barrier, inc=1, device_id=right, device_id_type=MESH)
+    for offset in range(1, tp_size):
+        pl.semaphore_signal(
+            barrier, inc=1, device_id=(ep, (tp + offset) % tp_size), device_id_type=MESH
+        )
 
     loads = []
     for expert in range(local_experts):
@@ -267,8 +280,9 @@
     ]
     for load in loads:
         load.start()
-
-    pl.semaphore_wait(barrier, ep_size + 1 + inner)
+    mix_own = pltpu.make_async_copy(mix_ref, mix.at[tp], mix_load)
+    mix_own.start()
+    pl.semaphore_wait(barrier, ep_size + tp_size - 2)
 
     def line_copy(source_ref, source, direction):
         return pltpu.make_async_remote_copy(
@@ -321,15 +335,116 @@
             device_id_type=MESH,
         )
 
-    def sum_copy(source, index, direction):
-        return pltpu.make_async_remote_copy(
-            src_ref=running.at[1 - direction, source, index],
-            dst_ref=running.at[1 - direction, source, index],
+    def sum_copy(source, place, index, direction):
+        return pltpu.make_async_remote_copy(
+            src_ref=running.at[source, index],
+            dst_ref=running.at[place, index],
             send_sem=(left_send, right_send)[direction].at[source, index],
             recv_sem=(right_recv, left_recv)[direction].at[source, index],
             device_id=(left, right)[direction],
             device_id_type=MESH,
         )
+
+    def sum_place(source, direction):
+        if direction == 1:
+            return source
+        ends = (source + 1) // jnp.maximum(z, 1)
+        return source + (planes - source) * ends
+
+    sequence, channels = pool_ref.shape
+    share_rows = sequence // tp_size
+    edge = halo.shape[0]
+
+    def halo_copy():
+        return pltpu.make_async_remote_copy(
+            src_ref=pool_ref.at[pl.ds(sequence - edge, edge)],
+            dst_ref=halo,
+            send_sem=halo_sems.at[0],
+            recv_sem=halo_sems.at[1],
+            device_id=peer_of(1),
+            device_id_type=MESH,
+        )
+
+    def pool_copy(offset):
+        target = (tp + offset) % tp_size
+        lanes = pl.ds(pl.multiple_of(tp * channels, channels), channels)
+        return pltpu.make_async_remote_copy(
+            src_ref=pooled.at[pl.ds(pl.multiple_of(target * share_rows, share_rows), share_rows)],
+            dst_ref=regrouped.at[:, lanes],
+            send_sem=pool_send.at[offset - 1],
+            recv_sem=pool_recv.at[offset - 1],
+            device_id=(ep, target),
+            device_id_type=MESH,
+        )
+
+    def mix_copy(offset):
+        return pltpu.make_async_remote_copy(
+            src_ref=mix.at[tp],
+            dst_ref=mix.at[tp],
+            send_sem=mix_send.at[offset - 1],
+            recv_sem=mix_recv.at[offset - 1],
+            device_id=(ep, (tp + 2 * offset) % tp_size),
+            device_id_type=MESH,
+        )
+
+    def pair_copy(offset):
+        block_of = (tp - 2 * offset + tp_size) % tp_size
+        return pltpu.make_async_remote_copy(
+            src_ref=mix.at[block_of],
+            dst_ref=mix.at[block_of],
+            send_sem=pair_send.at[offset],
+            recv_sem=pair_recv.at[offset],
+            device_id=partner,
+            device_id_type=MESH,
+        )
+
+    def pool():
+        @pl.when(ep > 0)
+        def _():
+            halo_copy().wait_recv()
+
+        before = jnp.where(ep > 0, halo[...].astype(jnp.float32), 0.0)
+        values = pool_ref[...].astype(jnp.float32)
+        level = jnp.concatenate([before, values], axis=0)
+        channel = tp * channels + lax.broadcasted_iota(jnp.int32, (1, channels), 1)
+        position = ep * sequence + lax.broadcasted_iota(jnp.int32, (sequence, 1), 0)
+        summed = jnp.zeros((sequence, channels), jnp.float32)
+        widths = jnp.zeros((1, channels), jnp.int32)
+        for index in range(4):
+            level = level + pltpu.roll(level, 2**index, 0)
+            inside = (channel >= index * GROUP_CH) & (channel < (index + 1) * GROUP_CH)
+            summed = jnp.where(inside, level[edge:], summed)
+            widths = jnp.where(inside, 2 ** (index + 1), widths)
+        counted = jnp.minimum(position + 1, widths).astype(jnp.float32)
+        result = (summed / counted - values) * gain_ref[...]
+        pooled[...] = result.astype(jnp.bfloat16)
+        own_rows = pl.ds(pl.multiple_of(tp * share_rows, share_rows), share_rows)
+        lanes = pl.ds(pl.multiple_of(tp * channels, channels), channels)
+        regrouped[:, lanes] = pooled[own_rows]
+
+    def send_mixer():
+        mix_own.wait()
+        for offset in range(1, tp_size):
+            pool_copy(offset).start()
+        for offset in range(1, planes):
+            mix_copy(offset).start()
+        pair_copy(0).start()
+
+    def pair_mixer():
+        for offset in range(1, planes):
+            mix_copy(offset).wait_recv()
+            pair_copy(offset).start()
+
+    def mixer():
+        for offset in range(1, tp_size):
+            pool_copy(offset).wait_recv()
+        for offset in range(planes):
+            pair_copy(offset).wait_recv()
+        total = jnp.zeros((share_rows, mix.shape[2]), jnp.float32)
+        for index in range(tp_size):
+            part = regrouped[:, index * channels : (index + 1) * channels]
+            total = total + jnp.dot(part, mix[index], preferred_element_type=jnp.float32)
+        mixed_ref[...] = total.astype(jnp.bfloat16)
 
     def dispatch(source_ref, source):
         routing = source_ref[:, width:].astype(jnp.float32).T
@@ -424,16 +539,17 @@
 
                 @pl.when(toward & has_before)
                 def _(direction=direction):
-                    before = sum_copy(source, index, direction)
-                    before.wait_recv()
-                    total = mine + running[1 - direction, source, index].astype(jnp.float32)
-                    running[1 - direction, source, index] = total.astype(jnp.bfloat16)
-                    sum_copy(source, index, direction).start()
+                    sum_copy(source, source, index, direction).wait_recv()
+                    total = mine + running[source, index].astype(jnp.float32)
+                    running[source, index] = total.astype(jnp.bfloat16)
+                    place = sum_place(source, direction)
+                    sum_copy(source, place, index, direction).start()
 
                 @pl.when(toward & ~has_before)
                 def _(direction=direction):
-                    running[1 - direction, source, index] = mine.astype(jnp.bfloat16)
-                    sum_copy(source, index, direction).start()
+                    running[source, index] = mine.astype(jnp.bfloat16)
+                    place = sum_place(source, direction)
+                    sum_copy(source, place, index, direction).start()
 
     @pl.when(has_left)
     def _():
@@ -443,7 +559,12 @@
     def _():
         line_copy(x_ref, z, 1).start()
 
+    @pl.when(ep < ep_size - 1)
+    def _():
+        halo_copy().start()
+
     dispatch(x_ref, z)
+    pool()
     for load in loads:
         load.wait()
 
@@ -463,6 +584,10 @@
 
             dispatch(column.at[source], source)
 
+        @pl.when(step == planes - 1)
+        def _():
+            send_mixer()
+
         previous = source_of(step - 1)
         slot = (step - 1) % 2
         gather(previous)
@@ -481,6 +606,7 @@
         return carry
 
     lax.fori_loop(1, planes + 1, step_body, 0)
+    pair_mixer()
 
     def tail_body(step, carry):
         @pl.when(~at_end | (step == planes - 1))
@@ -490,6 +616,7 @@
         return carry
 
     lax.fori_loop(1, planes, tail_body, 0)
+    mixer()
 
     placing = placing_back(x_ref)
     for index in range(PIECES):
@@ -501,11 +628,11 @@
 
             @pl.when(has_before)
             def _(direction=direction):
-                sum_copy(z, index, direction).wait_recv()
+                sum_copy(z, z, index, direction).wait_recv()
 
         zero = jnp.zeros_like(mine)
-        from_left = jnp.where(has_left, running[0, z, index].astype(jnp.float32), zero)
-        from_right = jnp.where(has_right, running[1, z, index].astype(jnp.float32), zero)
+        from_left = jnp.where(has_left, running[z, index].astype(jnp.float32), zero)
+        from_right = jnp.where(has_right, running[planes, index].astype(jnp.float32), zero)
         out_ref[:, lanes] = (mine + from_left + from_right).astype(jnp.bfloat16)
 
     @pl.when(has_left)
@@ -515,6 +642,17 @@
     @pl.when(has_right)
     def _():
         line_copy(x_ref, z, 1).wait_send()
+
+    @pl.when(ep < ep_size - 1)
+    def _():
+        halo_copy().wait_send()
+
+    for offset in range(1, tp_size):
+        pool_copy(offset).wait_send()
+    for offset in range(1, planes):
+        mix_copy(offset).wait_send()
+    for offset in range(planes):
+        pair_copy(offset).wait_send()
 
     def drain(source, carry):
         for offset in range(1, ep_size):
@@ -530,7 +668,7 @@
             @pl.when(toward)
             def _(direction=direction):
                 for index in range(PIECES):
-                    sum_copy(source, index, direction).wait_send()
+                    sum_copy(source, source, index, direction).wait_send()
 
             @pl.when(forwarded & has_next)
             def _(direction=direction):
@@ -544,8 +682,14 @@
             part_copy(0, slot, index).wait_send()
 
 
-def expert_layer(extended, gate_weight, up_weight, down_weight, ep_size, planes, slots):
+def fused_layers(extended, pool_input, pool_gain, mix_weight, weights, ep_size, planes, slots):
+    gate_weight, up_weight, down_weight = weights
     rows, wide = extended.shape
+    sequence, channels = pool_input.shape
+    depth, outputs = mix_weight.shape
+    tp_size = 2 * planes
+    share_rows = sequence // tp_size
+    edge = 16
     local_experts, width, ff = gate_weight.shape
     block = ep_size * slots
     piece = width // PIECES
@@ -553,9 +697,13 @@
     dma = pltpu.SemaphoreType.DMA
     return pl.pallas_call(
         functools.partial(expert_kernel, ep_size, planes),
-        out_shape=jax.ShapeDtypeStruct((rows, width), half),
-        in_specs=[pl.BlockSpec(memory_space=pltpu.VMEM)] + [pl.BlockSpec(memory_space=pl.ANY)] * 3,
-        out_specs=pl.BlockSpec(memory_space=pltpu.VMEM),
+        out_shape=(
+            jax.ShapeDtypeStruct((share_rows, outputs), half),
+            jax.ShapeDtypeStruct((rows, width), half),
+        ),
+        in_specs=[pl.BlockSpec(memory_space=pltpu.VMEM)] * 3
+        + [pl.BlockSpec(memory_space=pl.ANY)] * 4,
+        out_specs=(pl.BlockSpec(memory_space=pltpu.VMEM),) * 2,
         scratch_shapes=[
             pltpu.VMEM((planes, rows, wide), half),
             pltpu.VMEM((planes, ep_size - 1, slots, wide), half),
@@ -567,7 +715,7 @@
             pltpu.VMEM((planes, PIECES, block, piece), half),
             pltpu.VMEM((2, PIECES, block, piece), half),
             pltpu.VMEM((planes, PIECES, block, piece), half),
-            pltpu.VMEM((2, planes, PIECES, rows, piece), half),
+            pltpu.VMEM((planes + 1, PIECES, rows, piece), half),
             dma((3 * local_experts,)),
             dma((planes, 2)),
             dma((planes,)),
@@ -583,11 +731,23 @@
             dma((planes, PIECES)),
             dma((planes, PIECES)),
             dma((planes, PIECES)),
+            pltpu.VMEM((edge, channels), half),
+            pltpu.VMEM((sequence, channels), half),
+            pltpu.VMEM((share_rows, tp_size * channels), half),
+            pltpu.VMEM((tp_size, depth, outputs), half),
+            dma((2,)),
+            dma,
+            dma((tp_size - 1,)),
+            dma((tp_size - 1,)),
+            dma((planes - 1,)),
+            dma((planes - 1,)),
+            dma((planes,)),
+            dma((planes,)),
         ],
         compiler_params=pltpu.CompilerParams(
             collective_id=0, has_side_effects=True, vmem_limit_bytes=VMEM_LIMIT
         ),
-    )(extended, gate_weight, up_weight, down_weight)
+    )(extended, pool_input, pool_gain[None, :], mix_weight, gate_weight, up_weight, down_weight)
 
 
 def routing_lanes(expert_ids, route_weight, ep_size):
@@ -628,18 +788,20 @@
     scale_rows = lax.rsqrt(jnp.mean(inputs * inputs, axis=-1, keepdims=True) + eps_norm)
     normed = (inputs * scale_rows * moe_gain).astype(jnp.bfloat16)
     extended = jnp.concatenate([normed, routing_lanes(expert_ids, route_weight, ep_size)], axis=1)
-    moe_out = expert_layer(
-        extended, gate_weight, up_weight, down_weight, ep_size, planes, slots
+    return fused_layers(
+        extended,
+        pool_input,
+        pool_gain,
+        mix_weight,
+        (gate_weight, up_weight, down_weight),
+        ep_size,
+        planes,
+        slots,
     )
-    pooled = pool_mixer(pool_input, pool_gain)
-    mix_rows = lax.all_gather(mix_weight, "tp", axis=0, tiled=True)
-    regrouped = lax.all_to_all(pooled, "tp", split_axis=0, concat_axis=1, tiled=True)
-    mixed_out = jnp.dot(regrouped, mix_rows, preferred_element_type=jnp.float32)
-    return (mixed_out.astype(jnp.bfloat16), moe_out)
 
 
 def fits(mesh, shapes):
-    moe_input, gate_weight = shapes
+    pool_input, mix_weight, moe_input, gate_weight = shapes
     ep_size = mesh.shape["ep"]
     tp_size = mesh.shape["tp"]
     experts, width, ff = gate_weight
@@ -653,13 +815,20 @@
     slots = local_experts * CAP // TOP
     if slots % 16 or rows % 16:
         return False
-    needed = kernel_bytes(ep_size, tp_size // 2, rows, slots, width, ff, local_experts)
+    sequence = pool_input[0] // ep_size
+    channels = pool_input[1] // tp_size
+    share_rows = sequence // tp_size
+    if channels % LANES or mix_weight[0] != pool_input[1] or share_rows % 16 or mix_weight[1] % LANES:
+        return False
+    mixer = mix_weight[0] * mix_weight[1] + share_rows * (mix_weight[0] + mix_weight[1])
+    mixer += 2 * sequence * channels
+    needed = kernel_bytes(ep_size, tp_size // 2, rows, slots, width, ff, local_experts, mixer)
     return needed < VMEM_LIMIT
 
 
 def solution(mesh):
     def program(*arguments):
-        shapes = (arguments[3].shape, arguments[7].shape)
+        shapes = tuple(arguments[index].shape for index in (0, 2, 3, 7))
         body = fast_body if fits(mesh, shapes) else general_body
         return jax.shard_map(
             body,

time: 275 us -> 253 us (0.920)
  between operations: 14.2 us -> 0.67 us
  starting transfers between devices: 9.77 us -> 0 us
  Pallas kernels: 235 us -> 240 us
  matrix products: 3.81 us -> 0 us
    pallas_call x1, Pallas kernels: 235 us -> 240 us  [fused_layers(): pl.pallas_call(functools.partial(expert_kernel, ep_size, planes), out_sha...]
    all_to_all x1 -> x0, starting transfers between devices: 4.88 us -> none  [fast_body(): lax.all_to_all(pooled, 'tp', split_axis=0, concat_axis=1, tiled=True)]
    ppermute x1 -> x0, starting transfers between devices: 4.86 us -> none  [from_behind(): return lax.ppermute(shard, axis, pairs)]
    dot_general x1 -> x0, matrix products: 3.81 us -> none  [fast_body(): mixed_out = jnp.dot(regrouped, mix_rows, preferred_element_type=jnp.float32)]
  transfers between devices with their start and end apart: 3 -> 0, of which waited for: 0 -> 0; matrix products, arithmetic and copies ran while one was open for 4% -> 0% of each run, Pallas kernels for 85% -> 0%
where the time goes in v2:
time: 253 us; the launch traced here: 252 us
  Pallas kernels  240 us (95%)
  other arithmetic  6.91 us (3%)
  local copies, waits for them, and re-layouts  4.62 us (2%)
    pallas_call x1, Pallas kernels, fused_layers(): pl.pallas_call(functools.partial(expert_kernel, ep_size, planes), out_sha...  240 us

profile of v2, /device:TPU:0, one launch (start us, length us, event | category | flops | bytes accessed | tf_op | source)
XLA Modules:
  0.0 252.3 jit_solution(15392342118657686407)
XLA Ops:
  0.6 1.5 fusion.1
  2.1 0.7 and_select_fusion.1
  2.9 0.7 select_reduce_fusion
  3.6 1.2 reduce-window.6
  4.8 0.1 slice.8
  4.9 0.1 copy.25
  5.0 0.1 copy.26
  5.1 0.1 add_bitcast_fusion
  5.2 0.1 copy.27
  5.4 1.5 fusion.3
  6.9 1.1 fusion.4.x_ref
  8.0 240.1 %shard_map.113 = (bf16[128,2048]{1,0:T(8,128)(2,1)}, bf16[256,2048]{1,0:T(8,128)(2,1)}) custom-call(bf16[256,2176]{1,0:T(8,128)(2,1)} %fusion.4.x_ref, bf16[1024,128]{1,0:T(8,128)(2,1)} %pool_ref.1, f32[1,128]{1,0:T(1,128)} %bitcast.15, bf16[128,2048]{1,0:T(8,128)(2,1)} %mix_ref.1, bf16[4,2048,128]{2,1,0:T(8,128)(2,1)} %gate_ref.1, ...), custom_call_target="tpu_custom_call" | custom-call | tf_op jit(solution)/shard_map/pallas_call | solution.py:698
  248.1 1.9 copy.32
  250.0 2.3 copy.33
  (9 shorter events, 0.1 us)

commit v3 on v2

--- a/solution.py
+++ b/solution.py
@@ -377,26 +377,49 @@
             device_id_type=MESH,
         )
 
-    def mix_copy(offset):
+    def mix_copy(plane, direction):
         return pltpu.make_async_remote_copy(
-            src_ref=mix.at[tp],
-            dst_ref=mix.at[tp],
-            send_sem=mix_send.at[offset - 1],
-            recv_sem=mix_recv.at[offset - 1],
-            device_id=(ep, (tp + 2 * offset) % tp_size),
+            src_ref=mix.at[2 * plane + core],
+            dst_ref=mix.at[2 * plane + core],
+            send_sem=mix_send.at[plane, direction],
+            recv_sem=mix_recv.at[plane],
+            device_id=(left, right)[direction],
             device_id_type=MESH,
         )
 
-    def pair_copy(offset):
-        block_of = (tp - 2 * offset + tp_size) % tp_size
+    def pair_copy(plane):
         return pltpu.make_async_remote_copy(
-            src_ref=mix.at[block_of],
-            dst_ref=mix.at[block_of],
-            send_sem=pair_send.at[offset],
-            recv_sem=pair_recv.at[offset],
+            src_ref=mix.at[2 * plane + core],
+            dst_ref=mix.at[2 * plane + core],
+            send_sem=pair_send.at[plane],
+            recv_sem=pair_recv.at[plane],
             device_id=partner,
             device_id_type=MESH,
         )
+
+    def send_mix():
+        @pl.when(has_left)
+        def _():
+            mix_copy(z, 0).start()
+
+        @pl.when(has_right)
+        def _():
+            mix_copy(z, 1).start()
+
+        pair_copy(z).start()
+
+    def receive_mix(plane):
+        mix_copy(plane, 0).wait_recv()
+
+        @pl.when((plane > z) & has_left)
+        def _():
+            mix_copy(plane, 0).start()
+
+        @pl.when((plane < z) & has_right)
+        def _():
+            mix_copy(plane, 1).start()
+
+        pair_copy(plane).start()
 
     def pool():
         @pl.when(ep > 0)
@@ -422,24 +445,15 @@
         lanes = pl.ds(pl.multiple_of(tp * channels, channels), channels)
         regrouped[:, lanes] = pooled[own_rows]
 
-    def send_mixer():
-        mix_own.wait()
+    def send_pooled():
         for offset in range(1, tp_size):
             pool_copy(offset).start()
-        for offset in range(1, planes):
-            mix_copy(offset).start()
-        pair_copy(0).start()
-
-    def pair_mixer():
-        for offset in range(1, planes):
-            mix_copy(offset).wait_recv()
-            pair_copy(offset).start()
 
     def mixer():
         for offset in range(1, tp_size):
             pool_copy(offset).wait_recv()
-        for offset in range(planes):
-            pair_copy(offset).wait_recv()
+        for plane in range(planes):
+            pair_copy(plane).wait_recv()
         total = jnp.zeros((share_rows, mix.shape[2]), jnp.float32)
         for index in range(tp_size):
             part = regrouped[:, index * channels : (index + 1) * channels]
@@ -509,8 +523,11 @@
             partial[source, index] = total.astype(jnp.bfloat16)
             own_rows = pl.ds(pl.multiple_of(ep * slots, slots), slots)
             returned[source, index, own_rows] = partial[source, index, own_rows]
-            for offset in range(1, ep_size):
-                back_copy(source, offset, index).start()
+
+            @pl.when(source != z)
+            def _():
+                for offset in range(1, ep_size):
+                    back_copy(source, offset, index).start()
 
     def placing_back(source_ref):
         routing = source_ref[:, width:].astype(jnp.float32)
@@ -527,29 +544,32 @@
             back_copy(source, offset, index).wait_recv()
         return jnp.dot(placing, returned[source, index], preferred_element_type=jnp.float32)
 
-    def reduce_line(step):
-        source = sum_of(step)
-        placing = placing_back(column.at[source])
+    def reduce_piece(source, placing, index):
+        mine = combine(placing, source, index)
+        for direction in range(2):
+            toward = (source < z, source > z)[direction]
+            has_before = (has_right, has_left)[direction]
+
+            @pl.when(toward & has_before)
+            def _(direction=direction):
+                sum_copy(source, source, index, direction).wait_recv()
+                total = mine + running[source, index].astype(jnp.float32)
+                running[source, index] = total.astype(jnp.bfloat16)
+                place = sum_place(source, direction)
+                sum_copy(source, place, index, direction).start()
+
+            @pl.when(toward & ~has_before)
+            def _(direction=direction):
+                running[source, index] = mine.astype(jnp.bfloat16)
+                place = sum_place(source, direction)
+                sum_copy(source, place, index, direction).start()
+
+    def reduce_line(*steps):
+        sources = [sum_of(step) for step in steps]
+        placings = [placing_back(column.at[source]) for source in sources]
         for index in range(PIECES):
-            mine = combine(placing, source, index)
-
-            for direction in range(2):
-                toward = (source < z, source > z)[direction]
-                has_before = (has_right, has_left)[direction]
-
-                @pl.when(toward & has_before)
-                def _(direction=direction):
-                    sum_copy(source, source, index, direction).wait_recv()
-                    total = mine + running[source, index].astype(jnp.float32)
-                    running[source, index] = total.astype(jnp.bfloat16)
-                    place = sum_place(source, direction)
-                    sum_copy(source, place, index, direction).start()
-
-                @pl.when(toward & ~has_before)
-                def _(direction=direction):
-                    running[source, index] = mine.astype(jnp.bfloat16)
-                    place = sum_place(source, direction)
-                    sum_copy(source, place, index, direction).start()
+            for source, placing in zip(sources, placings):
+                reduce_piece(source, placing, index)
 
     @pl.when(has_left)
     def _():
@@ -558,6 +578,12 @@
     @pl.when(has_right)
     def _():
         line_copy(x_ref, z, 1).start()
+
+    mix_own.wait()
+
+    @pl.when(at_end)
+    def _():
+        send_mix()
 
     @pl.when(ep < ep_size - 1)
     def _():
@@ -568,30 +594,54 @@
     for load in loads:
         load.wait()
 
+    def receive(source):
+        line_copy(x_ref, source, 0).wait_recv()
+
+        @pl.when((source > z) & has_left)
+        def _():
+            line_copy(column.at[source], source, 0).start()
+
+        @pl.when((source < z) & has_right)
+        def _():
+            line_copy(column.at[source], source, 1).start()
+
     def step_body(step, carry):
+        current = source_of(step)
+
+        @pl.when((at_end & (step < planes)) | (~at_end & (step == 1)))
+        def _():
+            receive(current)
+
         @pl.when(step < planes)
         def _():
-            source = source_of(step)
-            line_copy(x_ref, source, 0).wait_recv()
-
-            @pl.when((source > z) & has_left)
-            def _():
-                line_copy(column.at[source], source, 0).start()
-
-            @pl.when((source < z) & has_right)
-            def _():
-                line_copy(column.at[source], source, 1).start()
-
-            dispatch(column.at[source], source)
-
-        @pl.when(step == planes - 1)
-        def _():
-            send_mixer()
+            dispatch(column.at[current], current)
+
+        @pl.when(~at_end & (step == 1))
+        def _():
+            receive(source_of(2))
+
+        @pl.when(at_end & (step == 2))
+        def _():
+            send_pooled()
 
         previous = source_of(step - 1)
         slot = (step - 1) % 2
         gather(previous)
 
+        @pl.when(~at_end & (step == 2))
+        def _():
+            receive(source_of(3))
+
+        @pl.when(~at_end & (step == planes))
+        def _():
+            send_mix()
+            send_pooled()
+            receive_mix(source_of(2))
+
+        @pl.when(at_end & (step == planes - 1))
+        def _():
+            reduce_line(1)
+
         @pl.when(step > 2)
         def _():
             for index in range(PIECES):
@@ -599,25 +649,29 @@
 
         experts(previous, slot)
 
-        @pl.when(at_end & (step > 2))
-        def _():
-            reduce_line(step - 2)
-
         return carry
 
     lax.fori_loop(1, planes + 1, step_body, 0)
-    pair_mixer()
-
-    def tail_body(step, carry):
-        @pl.when(~at_end | (step == planes - 1))
-        def _():
+    for index in range(PIECES):
+        for offset in range(1, ep_size):
+            back_copy(z, offset, index).start()
+
+    @pl.when(at_end)
+    def _():
+        for step in range(2, planes):
             reduce_line(step)
 
-        return carry
-
-    lax.fori_loop(1, planes, tail_body, 0)
+        for step in range(1, planes):
+            receive_mix(sum_of(step))
+
+    @pl.when(~at_end)
+    def _():
+        receive_mix(source_of(1))
+        receive_mix(source_of(3))
+        reduce_line(1)
+        reduce_line(2, 3)
+
     mixer()
-
     placing = placing_back(x_ref)
     for index in range(PIECES):
         mine = combine(placing, z, index)
@@ -649,10 +703,12 @@
 
     for offset in range(1, tp_size):
         pool_copy(offset).wait_send()
-    for offset in range(1, planes):
-        mix_copy(offset).wait_send()
-    for offset in range(planes):
-        pair_copy(offset).wait_send()
+    for direction in range(2):
+
+        @pl.when((has_left, has_right)[direction])
+        def _(direction=direction):
+            mix_copy(z, direction).wait_send()
+
 
     def drain(source, carry):
         for offset in range(1, ep_size):
@@ -660,6 +716,7 @@
             for index in range(PIECES):
                 back_copy(source, offset, index).wait_send()
         share_copy(source).wait_send()
+        pair_copy(source).wait_send()
         for direction in range(2):
             toward = (source < z, source > z)[direction]
             has_next = (has_left, has_right)[direction]
@@ -673,6 +730,7 @@
             @pl.when(forwarded & has_next)
             def _(direction=direction):
                 line_copy(x_ref, source, direction).wait_send()
+                mix_copy(source, direction).wait_send()
 
         return carry
 
@@ -739,8 +797,8 @@
             dma,
             dma((tp_size - 1,)),
             dma((tp_size - 1,)),
-            dma((planes - 1,)),
-            dma((planes - 1,)),
+            dma((planes, 2)),
+            dma((planes,)),
             dma((planes,)),
             dma((planes,)),
         ],

time: 253 us -> 202 us (0.80)
  Pallas kernels: 240 us -> 190 us
    pallas_call x1, Pallas kernels: 240 us -> 190 us  [fused_layers(): pl.pallas_call(functools.partial(expert_kernel, ep_size, planes), out_sha...]
where the time goes in v3:
time: 202 us
  Pallas kernels  190 us (94%)
  other arithmetic  6.91 us (3%)
  local copies, waits for them, and re-layouts  4.62 us (2%)
    pallas_call x1, Pallas kernels, fused_layers(): pl.pallas_call(functools.partial(expert_kernel, ep_size, planes), out_sha...  190 us
    unnamed x2, local copies, waits for them, and re-layouts  4.18 us

profile of v3, /device:TPU:0, one launch (start us, length us, event | category | flops | bytes accessed | tf_op | source)
XLA Modules:
  0.0 201.8 jit_solution(8168448805800743602)
XLA Ops:
  0.6 1.5 fusion.1
  2.1 0.7 and_select_fusion.1
  2.9 0.7 select_reduce_fusion
  3.6 1.2 reduce-window.6
  4.8 0.1 slice.8
  4.9 0.1 copy.25
  5.0 0.1 copy.26
  5.1 0.1 add_bitcast_fusion
  5.2 0.1 copy.27
  5.4 1.5 fusion.3
  6.9 1.1 fusion.4.x_ref
  8.0 189.6 %shard_map.113 = (bf16[128,2048]{1,0:T(8,128)(2,1)}, bf16[256,2048]{1,0:T(8,128)(2,1)}) custom-call(bf16[256,2176]{1,0:T(8,128)(2,1)} %fusion.4.x_ref, bf16[1024,128]{1,0:T(8,128)(2,1)} %pool_ref.1, f32[1,128]{1,0:T(1,128)} %bitcast.15, bf16[128,2048]{1,0:T(8,128)(2,1)} %mix_ref.1, bf16[4,2048,128]{2,1,0:T(8,128)(2,1)} %gate_ref.1, ...), custom_call_target="tpu_custom_call" | custom-call | tf_op jit(solution)/shard_map/pallas_call | solution.py:756
  197.6 1.9 copy.32
  199.5 2.3 %copy.33 = bf16[256,2048]{1,0:T(8,128)(2,1)} copy(bf16[256,2048]{1,0:T(8,128)(2,1)} %get-tuple-element.9) | data formatting | bytes 2097152
  (9 shorter events, 0.1 us)

commit v4 on v3

--- a/solution.py
+++ b/solution.py
@@ -224,6 +224,10 @@
     mix_load,
     pool_send,
     pool_recv,
+    block_send,
+    block_recv,
+    total_send,
+    total_recv,
     mix_send,
     mix_recv,
     pair_send,
@@ -250,11 +254,15 @@
 
     def source_of(step):
         both_ways = ((step + 1) // 2) * (2 * (step % 2) - 1)
-        offset = inner * both_ways + (1 - inner) * step
+        far_first = step + (step // 2) * (1 - 2 * (step % 2))
+        offset = inner * both_ways + (1 - inner) * far_first
         return (z + turn * offset + planes) % planes
 
-    def sum_of(step):
-        return (z + turn * step + planes) % planes
+    def is_end(source):
+        return (source * (planes - 1 - source)) == 0
+
+    def outward(source):
+        return 1 - 2 * (source // (planes // 2))
 
     def peer_of(offset):
         return ((ep + offset) % ep_size, tp)
@@ -350,6 +358,39 @@
             return source
         ends = (source + 1) // jnp.maximum(z, 1)
         return source + (planes - source) * ends
+
+    def block_copy(source, offset):
+        start = pl.multiple_of(((ep - offset + ep_size) % ep_size) * slots, slots)
+        return pltpu.make_async_remote_copy(
+            src_ref=tokens.at[source, core, pl.ds(start, slots)],
+            dst_ref=tokens.at[source, core, pl.ds(start, slots)],
+            send_sem=block_send.at[source, offset],
+            recv_sem=block_recv.at[source, offset],
+            device_id=(ep, tp + 2 * outward(source)),
+            device_id_type=MESH,
+        )
+
+    def half_rows(half):
+        return pl.ds(half * (block // 2), block // 2)
+
+    def total_copy(source, index, half):
+        hops = (z - source) * outward(source)
+        place = source + (planes - 1 - 2 * source) * ((planes - hops) // (planes - 1))
+        return pltpu.make_async_remote_copy(
+            src_ref=partial.at[source, index, half_rows(half)],
+            dst_ref=returned.at[place, index, half_rows(half)],
+            send_sem=total_send.at[source, 2 * index + half],
+            recv_sem=total_recv.at[source, 2 * index + half],
+            device_id=(ep, tp - 2 * outward(source)),
+            device_id_type=MESH,
+        )
+
+    def receive_block(source, offset):
+        block_copy(source, offset).wait_recv()
+
+        @pl.when(~at_end)
+        def _():
+            block_copy(source, offset).start()
 
     sequence, channels = pool_ref.shape
     share_rows = sequence // tp_size
@@ -484,6 +525,10 @@
             plane_copy(source, offset).wait_recv()
         share_copy(source).start()
 
+    def keep_own(source, index):
+        own_rows = pl.ds(pl.multiple_of(ep * slots, slots), slots)
+        returned[source, index, own_rows] = partial[source, index, own_rows]
+
     def experts(source, slot):
         share_copy(source).wait_recv()
 
@@ -521,13 +566,20 @@
             part_copy(source, slot, index).wait_recv()
             total = own + arriving[slot, index].astype(jnp.float32)
             partial[source, index] = total.astype(jnp.bfloat16)
-            own_rows = pl.ds(pl.multiple_of(ep * slots, slots), slots)
-            returned[source, index, own_rows] = partial[source, index, own_rows]
-
-            @pl.when(source != z)
+
+            @pl.when(~is_end(source))
+            def _():
+                keep_own(source, index)
+
+            @pl.when(~is_end(source))
             def _():
                 for offset in range(1, ep_size):
                     back_copy(source, offset, index).start()
+
+            @pl.when(is_end(source) & at_end & (source != z))
+            def _():
+                for half in range(2):
+                    total_copy(source, index, half).start()
 
     def placing_back(source_ref):
         routing = source_ref[:, width:].astype(jnp.float32)
@@ -564,137 +616,181 @@
                 place = sum_place(source, direction)
                 sum_copy(source, place, index, direction).start()
 
-    def reduce_line(*steps):
-        sources = [sum_of(step) for step in steps]
-        placings = [placing_back(column.at[source]) for source in sources]
+    def reduce_line(source):
+        placing = placing_back(column.at[source])
         for index in range(PIECES):
-            for source, placing in zip(sources, placings):
-                reduce_piece(source, placing, index)
-
-    @pl.when(has_left)
+            reduce_piece(source, placing, index)
+
+    def add_total(source, place, index, half):
+        total_copy(source, index, half).wait_recv()
+        which = half_rows(half)
+        total = partial[source, index, which].astype(jnp.float32)
+        total = total + returned[place, index, which].astype(jnp.float32)
+        partial[source, index, which] = total.astype(jnp.bfloat16)
+
+    def pass_total(source, index, half):
+        add_total(source, source, index, half)
+        total_copy(source, index, half).start()
+
+    def receive(source):
+        line_copy(x_ref, source, 0).wait_recv()
+
+        @pl.when((source > z) & has_left)
+        def _():
+            line_copy(column.at[source], source, 0).start()
+
+        @pl.when((source < z) & has_right)
+        def _():
+            line_copy(column.at[source], source, 1).start()
+
+    @pl.when(~at_end)
     def _():
         line_copy(x_ref, z, 0).start()
-
-    @pl.when(has_right)
-    def _():
         line_copy(x_ref, z, 1).start()
-
-    mix_own.wait()
-
-    @pl.when(at_end)
-    def _():
-        send_mix()
 
     @pl.when(ep < ep_size - 1)
     def _():
         halo_copy().start()
 
     dispatch(x_ref, z)
+
+    @pl.when(at_end)
+    def _():
+        block_copy(z, 0).start()
+
     pool()
+
+    @pl.when(at_end)
+    def _():
+        for offset in range(1, ep_size):
+            plane_copy(z, offset).wait_recv()
+            block_copy(z, offset).start()
+        share_copy(z).start()
+
+    mix_own.wait()
     for load in loads:
         load.wait()
 
-    def receive(source):
-        line_copy(x_ref, source, 0).wait_recv()
-
-        @pl.when((source > z) & has_left)
-        def _():
-            line_copy(column.at[source], source, 0).start()
-
-        @pl.when((source < z) & has_right)
-        def _():
-            line_copy(column.at[source], source, 1).start()
-
     def step_body(step, carry):
         current = source_of(step)
-
-        @pl.when((at_end & (step < planes)) | (~at_end & (step == 1)))
-        def _():
-            receive(current)
-
-        @pl.when(step < planes)
-        def _():
-            dispatch(column.at[current], current)
+        slot = step % 2
+
+        @pl.when(step == 0)
+        def _():
+            receive(source_of(1))
+            dispatch(column.at[source_of(1)], source_of(1))
+
+        @pl.when(at_end & (step == 1))
+        def _():
+            send_mix()
+            send_pooled()
+
+        @pl.when(at_end & (step == 2))
+        def _():
+            reduce_line(source_of(1))
+
+        @pl.when(~at_end & (step == 0))
+        def _():
+            receive_block(source_of(2), 0)
+            receive_block(source_of(2), 1)
 
         @pl.when(~at_end & (step == 1))
         def _():
-            receive(source_of(2))
-
-        @pl.when(at_end & (step == 2))
-        def _():
-            send_pooled()
-
-        previous = source_of(step - 1)
-        slot = (step - 1) % 2
-        gather(previous)
+            receive_block(source_of(2), 2)
+            receive_block(source_of(2), 3)
+            receive_block(source_of(3), 0)
+
+        @pl.when(~is_end(current))
+        def _():
+            gather(current)
+
+        @pl.when(~at_end & (step == 1))
+        def _():
+            receive_block(source_of(3), 1)
 
         @pl.when(~at_end & (step == 2))
         def _():
-            receive(source_of(3))
-
-        @pl.when(~at_end & (step == planes))
-        def _():
+            receive_block(source_of(3), 2)
+
+        @pl.when(~at_end & (step == 3))
+        def _():
+            receive_block(source_of(3), 3)
             send_mix()
             send_pooled()
             receive_mix(source_of(2))
 
-        @pl.when(at_end & (step == planes - 1))
-        def _():
-            reduce_line(1)
-
-        @pl.when(step > 2)
+        @pl.when(at_end & (step == 2))
+        def _():
+            for offset in range(ep_size):
+                receive_block(current, offset)
+
+        @pl.when(is_end(current) & (current != z))
+        def _():
+            share_copy(current).start()
+
+        @pl.when(step > 1)
         def _():
             for index in range(PIECES):
-                part_copy(previous, slot, index).wait_send()
-
-        experts(previous, slot)
+                part_copy(current, slot, index).wait_send()
+
+        experts(current, slot)
+
+        @pl.when(at_end & (step == 1))
+        def _():
+            receive(source_of(3))
+            dispatch(column.at[source_of(3)], source_of(3))
 
         return carry
 
-    lax.fori_loop(1, planes + 1, step_body, 0)
-    for index in range(PIECES):
-        for offset in range(1, ep_size):
-            back_copy(z, offset, index).start()
+    lax.fori_loop(0, planes, step_body, 0)
 
     @pl.when(at_end)
     def _():
-        for step in range(2, planes):
-            reduce_line(step)
-
+        for index in range(PIECES - 1):
+            for half in range(2):
+                total_copy(source_of(2), index, half).wait_send()
+        reduce_line(source_of(3))
         for step in range(1, planes):
-            receive_mix(sum_of(step))
+            receive_mix(source_of(step))
+        for index in range(PIECES):
+            for half in range(2):
+                add_total(z, planes - 1 - z, index, half)
+            keep_own(z, index)
+            for offset in range(1, ep_size):
+                back_copy(z, offset, index).start()
 
     @pl.when(~at_end)
     def _():
         receive_mix(source_of(1))
         receive_mix(source_of(3))
-        reduce_line(1)
-        reduce_line(2, 3)
+        for index in range(PIECES):
+            for half in range(2):
+                pass_total(source_of(3), index, half)
+                pass_total(source_of(2), index, half)
+        reduce_line(source_of(1))
 
     mixer()
+
     placing = placing_back(x_ref)
     for index in range(PIECES):
         mine = combine(placing, z, index)
         lanes = pl.ds(index * piece, piece)
 
-        for direction in range(2):
-            has_before = (has_right, has_left)[direction]
-
-            @pl.when(has_before)
-            def _(direction=direction):
-                sum_copy(z, z, index, direction).wait_recv()
-
-        zero = jnp.zeros_like(mine)
-        from_left = jnp.where(has_left, running[z, index].astype(jnp.float32), zero)
-        from_right = jnp.where(has_right, running[planes, index].astype(jnp.float32), zero)
-        out_ref[:, lanes] = (mine + from_left + from_right).astype(jnp.bfloat16)
-
-    @pl.when(has_left)
+        @pl.when(~at_end)
+        def _():
+            sum_copy(z, z, index, 0).wait_recv()
+            sum_copy(z, z, index, 1).wait_recv()
+            others = running[z, index].astype(jnp.float32)
+            others = others + running[planes, index].astype(jnp.float32)
+            out_ref[:, lanes] = (mine + others).astype(jnp.bfloat16)
+
+        @pl.when(at_end)
+        def _():
+            out_ref[:, lanes] = mine.astype(jnp.bfloat16)
+
+    @pl.when(~at_end)
     def _():
         line_copy(x_ref, z, 0).wait_send()
-
-    @pl.when(has_right)
-    def _():
         line_copy(x_ref, z, 1).wait_send()
 
     @pl.when(ep < ep_size - 1)
@@ -711,25 +807,48 @@
 
 
     def drain(source, carry):
-        for offset in range(1, ep_size):
-            plane_copy(source, offset).wait_send()
-            for index in range(PIECES):
-                back_copy(source, offset, index).wait_send()
+        @pl.when(~is_end(source) | (source == z))
+        def _():
+            for offset in range(1, ep_size):
+                plane_copy(source, offset).wait_send()
+                for index in range(PIECES):
+                    back_copy(source, offset, index).wait_send()
+
         share_copy(source).wait_send()
         pair_copy(source).wait_send()
+
+        @pl.when(is_end(source) & (~at_end | (source == z)))
+        def _():
+            for offset in range(ep_size):
+                block_copy(source, offset).wait_send()
+
+        @pl.when(is_end(source) & (source != z))
+        def _():
+            @pl.when(~at_end)
+            def _():
+                for index in range(PIECES - 1):
+                    for half in range(2):
+                        total_copy(source, index, half).wait_send()
+
+            for half in range(2):
+                total_copy(source, PIECES - 1, half).wait_send()
+
         for direction in range(2):
             toward = (source < z, source > z)[direction]
             has_next = (has_left, has_right)[direction]
             forwarded = (source > z, source < z)[direction]
 
-            @pl.when(toward)
+            @pl.when(~is_end(source) & toward)
             def _(direction=direction):
                 for index in range(PIECES):
                     sum_copy(source, source, index, direction).wait_send()
 
+            @pl.when(~is_end(source) & forwarded & has_next)
+            def _(direction=direction):
+                line_copy(x_ref, source, direction).wait_send()
+
             @pl.when(forwarded & has_next)
             def _(direction=direction):
-                line_copy(x_ref, source, direction).wait_send()
                 mix_copy(source, direction).wait_send()
 
         return carry
@@ -797,6 +916,10 @@
             dma,
             dma((tp_size - 1,)),
             dma((tp_size - 1,)),
+            dma((planes, ep_size)),
+            dma((planes, ep_size)),
+            dma((planes, 2 * PIECES)),
+            dma((planes, 2 * PIECES)),
             dma((planes, 2)),
             dma((planes,)),
             dma((planes,)),
@@ -866,7 +989,7 @@
     local_experts = experts // ep_size
     rows = moe_input[0] // (ep_size * tp_size)
     ff = ff // tp_size
-    if local_experts % GROUP_EXP or tp_size % 4 or tp_size > 8 or ff % LANES or width % (PIECES * LANES):
+    if local_experts % GROUP_EXP or tp_size != 8 or ep_size != 4 or ff % LANES or width % (PIECES * LANES):
         return False
     if 2 * local_experts + ep_size > LANES or rows > 256:
         return False

time: 202 us -> 195 us (0.965)
  the two profiles are of different devices: /device:TPU:0 before, /device:TPU:8 now
where the time goes in v4:
time: 195 us
  Pallas kernels  183 us (94%)
  other arithmetic  6.91 us (4%)
  local copies, waits for them, and re-layouts  4.62 us (2%)
    pallas_call x1, Pallas kernels, fused_layers(): pl.pallas_call(functools.partial(expert_kernel, ep_size, planes), out_sha...  183 us
    unnamed x2, local copies, waits for them, and re-layouts  4.18 us

profile of v4, /device:TPU:8, one launch (start us, length us, event | category | flops | bytes accessed | tf_op | source)
XLA Modules:
  0.0 194.9 jit_solution(14577652933983142764)
XLA Ops:
  0.6 1.5 fusion.1
  2.1 0.7 and_select_fusion.1
  2.9 0.7 select_reduce_fusion
  3.6 1.2 reduce-window.6
  4.8 0.1 slice.8
  4.9 0.1 copy.25
  5.0 0.1 copy.26
  5.1 0.1 add_bitcast_fusion
  5.2 0.1 copy.27
  5.4 1.5 fusion.3
  6.9 1.1 fusion.4.x_ref
  8.0 182.7 %shard_map.113 = (bf16[128,2048]{1,0:T(8,128)(2,1)}, bf16[256,2048]{1,0:T(8,128)(2,1)}) custom-call(bf16[256,2176]{1,0:T(8,128)(2,1)} %fusion.4.x_ref, bf16[1024,128]{1,0:T(8,128)(2,1)} %pool_ref.1, f32[1,128]{1,0:T(1,128)} %bitcast.15, bf16[128,2048]{1,0:T(8,128)(2,1)} %mix_ref.1, bf16[4,2048,128]{2,1,0:T(8,128)(2,1)} %gate_ref.1, ...), custom_call_target="tpu_custom_call" | custom-call | tf_op jit(solution)/shard_map/pallas_call | solution.py:875
  190.7 1.9 copy.32
  192.6 2.3 %copy.33 = bf16[256,2048]{1,0:T(8,128)(2,1)} copy(bf16[256,2048]{1,0:T(8,128)(2,1)} %get-tuple-element.9) | data formatting | bytes 2097152
  (9 shorter events, 0.1 us)

commit v5 on v4

--- a/solution.py
+++ b/solution.py
@@ -159,6 +159,7 @@
 
 LANES = 128
 PIECES = 4
+LAG = 2
 VMEM_LIMIT = 67043328
 MESH = pl.DeviceIdType.MESH
 
@@ -181,7 +182,9 @@
 def expert_kernel(
     ep_size,
     planes,
-    x_ref,
+    input_ref,
+    scale_ref,
+    routes_ref,
     pool_ref,
     gain_ref,
     mix_ref,
@@ -237,8 +240,9 @@
     tp = lax.axis_index("tp")
     z = tp // 2
     core = tp % 2
-    rows, wide = x_ref.shape
-    local_experts, width, ff = gate_ref.shape
+    rows, width = input_ref.shape
+    wide = width + LANES
+    local_experts, _, ff = gate_ref.shape
     slots = packed.shape[2]
     block = ep_size * slots
     piece = width // PIECES
@@ -290,6 +294,44 @@
         load.start()
     mix_own = pltpu.make_async_copy(mix_ref, mix.at[tp], mix_load)
     mix_own.start()
+    x_ref = column.at[z]
+
+    def normalize():
+        values = input_ref[...].astype(jnp.float32)
+        mean = jnp.mean(values * values, axis=-1, keepdims=True)
+        values = values * lax.rsqrt(mean + eps_norm) * scale_ref[...]
+        column[z, :, :width] = values.astype(jnp.bfloat16)
+
+    def route():
+        routes = routes_ref[...].T
+        lane = lax.broadcasted_iota(jnp.int32, (rows, LANES), 1)
+        place = (lane - 2 * local_experts).astype(jnp.float32)
+        inside = (place >= 0) & (place < ep_size)
+        within = jnp.where(lane < local_experts, lane, lane - local_experts).astype(jnp.float32)
+        named = jnp.zeros((rows, LANES), jnp.float32)
+        weights = jnp.zeros((rows, LANES), jnp.float32)
+        for index in range(TOP):
+            expert = routes[:, index : index + 1]
+            weight = routes[:, TOP + index : TOP + index + 1]
+            first = place * local_experts
+            here = (expert >= first) & (expert < first + local_experts) & inside
+            named = jnp.where(here, 1.0, named)
+            for group in range(ep_size):
+                chosen = expert == within + group * local_experts
+                weights = weights + jnp.where(chosen, weight, 0.0)
+        earlier = lax.broadcasted_iota(jnp.int32, (rows, rows), 1)
+        later = lax.broadcasted_iota(jnp.int32, (rows, rows), 0)
+        before = jnp.where(earlier < later, 1.0, 0.0).astype(jnp.bfloat16)
+        rank = jnp.dot(before, named.astype(jnp.bfloat16), preferred_element_type=jnp.float32)
+        slot = jnp.where(named > 0.5, rank, -1.0)
+        high = weights.astype(jnp.bfloat16).astype(jnp.float32)
+        lanes = jnp.where(inside, slot, 0.0)
+        lanes = jnp.where(lane < 2 * local_experts, weights - high, lanes)
+        lanes = jnp.where(lane < local_experts, high, lanes)
+        column[z, :, width:] = lanes.astype(jnp.bfloat16)
+
+    normalize()
+    route()
     pl.semaphore_wait(barrier, ep_size + tp_size - 2)
 
     def line_copy(source_ref, source, direction):
@@ -746,9 +788,6 @@
 
     @pl.when(at_end)
     def _():
-        for index in range(PIECES - 1):
-            for half in range(2):
-                total_copy(source_of(2), index, half).wait_send()
         reduce_line(source_of(3))
         for step in range(1, planes):
             receive_mix(source_of(step))
@@ -763,10 +802,11 @@
     def _():
         receive_mix(source_of(1))
         receive_mix(source_of(3))
-        for index in range(PIECES):
-            for half in range(2):
-                pass_total(source_of(3), index, half)
-                pass_total(source_of(2), index, half)
+        for count in range(2 * PIECES + LAG):
+            if count < 2 * PIECES:
+                pass_total(source_of(3), count // 2, count % 2)
+            if count >= LAG:
+                pass_total(source_of(2), (count - LAG) // 2, (count - LAG) % 2)
         reduce_line(source_of(1))
 
     mixer()
@@ -824,14 +864,9 @@
 
         @pl.when(is_end(source) & (source != z))
         def _():
-            @pl.when(~at_end)
-            def _():
-                for index in range(PIECES - 1):
-                    for half in range(2):
-                        total_copy(source, index, half).wait_send()
-
-            for half in range(2):
-                total_copy(source, PIECES - 1, half).wait_send()
+            for index in range(PIECES):
+                for half in range(2):
+                    total_copy(source, index, half).wait_send()
 
         for direction in range(2):
             toward = (source < z, source > z)[direction]
@@ -859,15 +894,17 @@
             part_copy(0, slot, index).wait_send()
 
 
-def fused_layers(extended, pool_input, pool_gain, mix_weight, weights, ep_size, planes, slots):
+def fused_layers(tokens, pool_input, pool_gain, mix_weight, weights, ep_size, planes, slots):
     gate_weight, up_weight, down_weight = weights
-    rows, wide = extended.shape
+    moe_input, moe_gain, routes = tokens
+    rows, width = moe_input.shape
+    wide = width + LANES
     sequence, channels = pool_input.shape
     depth, outputs = mix_weight.shape
     tp_size = 2 * planes
     share_rows = sequence // tp_size
     edge = 16
-    local_experts, width, ff = gate_weight.shape
+    local_experts, _, ff = gate_weight.shape
     block = ep_size * slots
     piece = width // PIECES
     half = jnp.bfloat16
@@ -878,7 +915,7 @@
             jax.ShapeDtypeStruct((share_rows, outputs), half),
             jax.ShapeDtypeStruct((rows, width), half),
         ),
-        in_specs=[pl.BlockSpec(memory_space=pltpu.VMEM)] * 3
+        in_specs=[pl.BlockSpec(memory_space=pltpu.VMEM)] * 5
         + [pl.BlockSpec(memory_space=pl.ANY)] * 4,
         out_specs=(pl.BlockSpec(memory_space=pltpu.VMEM),) * 2,
         scratch_shapes=[
@@ -928,25 +965,17 @@
         compiler_params=pltpu.CompilerParams(
             collective_id=0, has_side_effects=True, vmem_limit_bytes=VMEM_LIMIT
         ),
-    )(extended, pool_input, pool_gain[None, :], mix_weight, gate_weight, up_weight, down_weight)
-
-
-def routing_lanes(expert_ids, route_weight, ep_size):
-    local_experts = EXPERTS // ep_size
-    owners = expert_ids // local_experts
-    ep_index = lax.iota(jnp.int32, ep_size)
-    member = jnp.any(owners[:, :, None] == ep_index[None, None, :], axis=1)
-    counts = member.astype(jnp.int32)
-    rank = jnp.cumsum(counts, axis=0) - counts
-    slot = jnp.where(member, rank, -1).astype(jnp.float32)
-    within = expert_ids % local_experts
-    named = within[:, :, None] == lax.iota(jnp.int32, local_experts)[None, None, :]
-    weights = jnp.sum(jnp.where(named, route_weight[:, :, None], 0.0), axis=1)
-    high = lax.reduce_precision(weights, 8, 7)
-    low = weights - high
-    spare = LANES - 2 * local_experts - ep_size
-    lanes = jnp.concatenate([high, low, slot], axis=1)
-    return jnp.pad(lanes, ((0, 0), (0, spare))).astype(jnp.bfloat16)
+    )(
+        moe_input,
+        moe_gain[None, :],
+        routes,
+        pool_input,
+        pool_gain[None, :],
+        mix_weight,
+        gate_weight,
+        up_weight,
+        down_weight,
+    )
 
 
 def fast_body(
@@ -965,12 +994,10 @@
     planes = lax.axis_size("tp") // 2
     local_experts = gate_weight.shape[0]
     slots = local_experts * CAP // TOP
-    inputs = moe_input.astype(jnp.float32)
-    scale_rows = lax.rsqrt(jnp.mean(inputs * inputs, axis=-1, keepdims=True) + eps_norm)
-    normed = (inputs * scale_rows * moe_gain).astype(jnp.bfloat16)
-    extended = jnp.concatenate([normed, routing_lanes(expert_ids, route_weight, ep_size)], axis=1)
+    routes = jnp.concatenate([expert_ids.T.astype(jnp.float32), route_weight.T], axis=0)
+    routes = jnp.pad(routes, ((0, 8 - 2 * TOP), (0, 0)))
     return fused_layers(
-        extended,
+        (moe_input, moe_gain, routes),
         pool_input,
         pool_gain,
         mix_weight,

time: 195 us -> 182 us (0.933)
  the two profiles are of different devices: /device:TPU:8 before, /device:TPU:0 now
where the time goes in v5:
time: 182 us
  Pallas kernels  175 us (96%)
  local copies, waits for them, and re-layouts  4.18 us (2%)
  other arithmetic  1.97 us (1%)
    pallas_call x1, Pallas kernels, fused_layers(): pl.pallas_call(functools.partial(expert_kernel, ep_size, planes), out_sha...  175 us
    unnamed x2, local copies, waits for them, and re-layouts  4.18 us

profile of v5, /device:TPU:0, one launch (start us, length us, event | category | flops | bytes accessed | tf_op | source)
XLA Modules:
  0.0 181.5 jit_solution(3840740943192416653)
XLA Ops:
  0.6 0.7 convert_bitcast_fusion
  1.3 1.3 select_maximum_fusion.routes_ref
  2.6 174.7 %shard_map.113 = (bf16[128,2048]{1,0:T(8,128)(2,1)}, bf16[256,2048]{1,0:T(8,128)(2,1)}) custom-call(bf16[256,2048]{1,0:T(8,128)(2,1)} %input_ref.1, f32[1,2048]{1,0:T(1,128)} %bitcast.5, f32[8,256]{1,0:T(8,128)} %select_maximum_fusion.routes_ref, bf16[1024,128]{1,0:T(8,128)(2,1)} %pool_ref.1, f32[1,128]{1,0:T(1,128)} %bitcast.7, bf16[128,2048]{1,0:T(8,128)(2,1)} %mix_ref.1, ...), custom_call_target="tpu_custom_call" | custom-call | tf_op jit(solution)/shard_map/pallas_call | solution.py:912
  177.4 1.9 %copy.14 = bf16[128,2048]{1,0:T(8,128)(2,1)} copy(bf16[128,2048]{1,0:T(8,128)(2,1)} %get-tuple-element.4) | data formatting | bytes 1048576
  179.2 2.3 %copy.15 = bf16[256,2048]{1,0:T(8,128)(2,1)} copy(bf16[256,2048]{1,0:T(8,128)(2,1)} %get-tuple-element.5) | data formatting | bytes 2097152
